TPU v7x, 32 devices: a whole 2x2x4 slice. The times are simulated.
32 devices in a mesh: sp: 8 (over z, y), tp: 4 (over x, core).
Axes of the slice: x: 2, y: 2, z: 4, core: 2. Of those that a mesh axis runs over, the one named last changes fastest.
Arguments:
- query_first: bfloat16 [2048, 512], P('sp', 'tp'), may hold values from -6 to 6
- key_first: bfloat16 [2048, 512], P('sp', 'tp'), may hold values from -6 to 6
- value_first: bfloat16 [2048, 1024], P('sp', 'tp'), may hold values from -6 to 6
- decay_first: float32 [2048, 512], P('sp', 'tp'), may hold values from -1 to 0
- gate_first: bfloat16 [2048, 1024], P('sp', 'tp'), may hold values from -6 to 6
- norm_first: float32 [256], replicated, may hold values from 0.1 to 1.9
- proj_first: bfloat16 [1024, 2048], P('tp', 'sp'), may hold values from -0.125 to 0.125
- query_second: bfloat16 [2048, 512], P('sp', 'tp'), may hold values from -6 to 6
- key_second: bfloat16 [2048, 512], P('sp', 'tp'), may hold values from -6 to 6
- value_second: bfloat16 [2048, 1024], P('sp', 'tp'), may hold values from -6 to 6
- decay_second: float32 [2048, 512], P('sp', 'tp'), may hold values from -1 to 0
- gate_second: bfloat16 [2048, 1024], P('sp', 'tp'), may hold values from -6 to 6
- norm_second: float32 [128], replicated, may hold values from 0.1 to 1.9
- proj_second: bfloat16 [1024, 2048], P('tp', 'sp'), may hold values from -0.125 to 0.125
- residual_in: bfloat16 [2048, 2048], P(('sp', 'tp')), may hold values from -6 to 6
- expert_norm: float32 [2048], replicated, may hold values from 0.1 to 1.9
- route_ids: int32 [2048, 2], P('sp'), may hold values from 0 to 7, all different within a row; in each aligned block of 256 rows (0 to 255, 256 to 511, ...) at most 128 rows name the same one
- route_weight: float32 [2048, 2], P('sp'), may hold values from 0.1 to 0.9
- expert_gate: bfloat16 [8, 2048, 3584], P('sp', None, 'tp'), may hold values from -0.125 to 0.125
- expert_up: bfloat16 [8, 2048, 3584], P('sp', None, 'tp'), may hold values from -0.125 to 0.125
- expert_down: bfloat16 [8, 3584, 2048], P('sp', 'tp'), may hold values from -0.09375 to 0.09375
Outputs:
- layer_out: bfloat16 [2048, 2048], P(('sp', 'tp'))
Inputs may be any that keep to these rules, and one draw needn't show every extreme that they name: `route_ids`: each row names 2 different experts. Among the 256 rows of one index of sp no expert is named by more than 128 rows, and in every draw some expert is named by exactly 128 of them.
All inputs are finite; a program needn't handle non-finite values.
Results may differ from a plain program's by a relative error of at most 0.015.
Values may be sent and summed in bfloat16 or wider, within the bound.
A program may use at most 64 MiB of HBM per device.

v0:
```python
import functools

import jax
import jax.numpy as jnp
from jax import lax
from jax.experimental import pallas as pl
from jax.experimental.pallas import tpu as pltpu
from jax.sharding import PartitionSpec as P

KA = 128
VA = 256
KB = 64
VB = 128
BLK = 64
PAIR = 2


epsilon = 1e-06
highest = lax.Precision.HIGHEST
MESH = pl.DeviceIdType.MESH
VMEM = pl.BlockSpec(memory_space=pltpu.VMEM)


def greet(peers):
    barrier = pltpu.get_barrier_semaphore()
    for peer in peers:
        pl.semaphore_signal(barrier, inc=1, device_id=peer, device_id_type=MESH)
    pl.semaphore_wait(barrier, len(peers))


def group_member(axis, span, step):
    me = lax.axis_index(axis)
    inside = lax.rem(me, span)
    other = lax.rem(inside + step, span)
    return inside, other, {axis: me - inside + other}


def exchange_kernel(axis, span, spread, count, *refs):
    sources, targets = refs[:count], refs[count : 2 * count]
    send_sems, recv_sems = refs[2 * count :]
    greet([group_member(axis, span, step)[2] for step in range(1, span)])
    copies = []
    for step in range(1, span):
        inside, other, device = group_member(axis, span, step)
        for i in range(count):
            copy = pltpu.make_async_remote_copy(
                src_ref=sources[i].at[other] if spread else sources[i],
                dst_ref=targets[i].at[inside],
                send_sem=send_sems.at[i, step],
                recv_sem=recv_sems.at[i, step],
                device_id=device,
                device_id_type=MESH,
            )
            copy.start()
            copies.append(copy)
    inside = lax.rem(lax.axis_index(axis), span)
    for i in range(count):
        targets[i][inside] = sources[i][inside] if spread else sources[i][...]
    for copy in copies:
        copy.wait()


def exchange(arrays, axis, span, spread, number):
    shapes = tuple(
        jax.ShapeDtypeStruct(a.shape if spread else (span,) + a.shape, a.dtype) for a in arrays
    )
    count = len(arrays)
    return pl.pallas_call(
        functools.partial(exchange_kernel, axis, span, spread, count),
        out_shape=shapes,
        in_specs=[VMEM] * count,
        out_specs=(VMEM,) * count,
        scratch_shapes=[
            pltpu.SemaphoreType.DMA((count, span)),
            pltpu.SemaphoreType.DMA((count, span)),
        ],
        compiler_params=pltpu.CompilerParams(collective_id=number, has_side_effects=True),
    )(*arrays)


def tp_member(across, sibling):
    size, me = lax.axis_size("tp"), lax.axis_index("tp")
    seat = lax.rem(me, PAIR)
    base = lax.rem(me - seat + across * PAIR, size)
    return base + (lax.rem(seat + 1, PAIR) if sibling else seat)


def remote(source, target, sems, index, device):
    return pltpu.make_async_remote_copy(
        src_ref=source,
        dst_ref=target,
        send_sem=sems[0].at[index],
        recv_sem=sems[1].at[index],
        device_id=device,
        device_id_type=MESH,
    )


def gather_kernel(size, pairs, spread, source, target, *sems):
    sp_sems, pair_sems, far_sems = sems[:2], sems[2:4], sems[4:]
    me, mine = lax.axis_index("sp"), lax.axis_index("tp")
    sibling = {"tp": tp_member(0, True)}
    far = [{"tp": tp_member(across, False)} for across in range(1, pairs)]
    peers = [group_member("sp", size, step) for step in range(1, size)] if spread else []
    greet([peer[2] for peer in peers] + [sibling] + far)
    copies = []
    for step, (_, other, device) in enumerate(peers, 1):
        copies.append(remote(source.at[other], target.at[mine, me], sp_sems, step, device))
        copies[-1].start()
    passed, distant = [], []
    for step in range(size):
        if spread:
            origin = lax.rem(me - step + size, size)
        else:
            origin = step
        own = step == 0 or not spread
        if not own:
            copies[step - 1].wait_recv()
        block = source.at[origin] if own else target.at[mine, origin]
        for across in range(1, pairs):
            copy = remote(
                block, target.at[mine, origin], far_sems, (across, step), far[across - 1]
            )
            copy.start()
            distant.append((copy, tp_member(pairs - across, False), origin, across, step))
        copy = remote(block, target.at[mine, origin], pair_sems, (0, step), sibling)
        copy.start()
        passed.append(copy)
        if own:
            target[mine, origin] = source[origin]
    for copy, sender, origin, across, step in distant:
        copy.wait_recv()
        block = target.at[sender, origin]
        again = remote(block, block, pair_sems, (across, step), sibling)
        again.start()
        passed.append(again)
    for copy in copies + [item[0] for item in distant]:
        copy.wait_send()
    for copy in passed:
        copy.wait()


def gather_tp(blocks, spread, number):
    size, tp = blocks.shape[0], lax.axis_size("tp")
    pairs = tp // PAIR
    return pl.pallas_call(
        functools.partial(gather_kernel, size, pairs, spread),
        out_shape=jax.ShapeDtypeStruct((tp,) + blocks.shape, blocks.dtype),
        in_specs=[VMEM],
        out_specs=VMEM,
        scratch_shapes=[pltpu.SemaphoreType.DMA((size,))] * 2
        + [pltpu.SemaphoreType.DMA((pairs, size))] * 4,
        compiler_params=pltpu.CompilerParams(collective_id=number, has_side_effects=True),
    )(blocks)


def reduce_kernel(size, pairs, spread, source, target, near, paired, arrived, *rest):
    done = rest[0] if spread else None
    sems = rest[1:] if spread else rest
    pair_sems, far_sems, sp_sems = sems[:2], sems[2:4], sems[4:]
    me = lax.axis_index("sp")
    sibling = {"tp": tp_member(0, True)}
    far = [{"tp": tp_member(across, False)} for across in range(1, pairs)]
    peers = [group_member("sp", size, step) for step in range(1, size)] if spread else []
    greet([peer[2] for peer in peers] + [sibling] + far)
    order = [lax.rem(me + k + 1, size) if spread else k for k in range(size)]
    hops = list(range(1, pairs)) + [0]
    first = {}
    for k in range(size):
        for across in hops:
            copy = remote(
                source.at[tp_member(across, True), order[k]],
                near.at[across, order[k]],
                pair_sems,
                (across, k),
                sibling,
            )
            copy.start()
            first[k, across] = copy
    second = {}
    for k in range(size):
        for across in hops:
            first[k, across].wait_recv()
            total = source[tp_member(across, False), order[k]].astype(jnp.float32)
            total = total + near[across, order[k]].astype(jnp.float32)
            paired[across, order[k]] = total.astype(paired.dtype)
        for across in range(1, pairs):
            copy = remote(
                paired.at[across, order[k]],
                arrived.at[across, order[k]],
                far_sems,
                (across, k),
                far[across - 1],
            )
            copy.start()
            second[k, across] = copy
    third = []
    for k in range(size):
        total = paired[0, order[k]].astype(jnp.float32)
        for across in range(1, pairs):
            second[k, across].wait_recv()
            total = total + arrived[across, order[k]].astype(jnp.float32)
        if not spread:
            target[order[k]] = total
        elif k == size - 1:
            target[me] = total.astype(target.dtype)
        else:
            done[order[k]] = total.astype(done.dtype)
            copy = remote(done.at[order[k]], target.at[me], sp_sems, k, peers[k][2])
            copy.start()
            third.append(copy)
    for copy in list(first.values()) + list(second.values()):
        copy.wait_send()
    for copy in third:
        copy.wait()


def reduce_tp(blocks, spread, number):
    tp, size, rows, width = blocks.shape
    pairs = tp // PAIR
    kept = pltpu.VMEM((pairs, size, rows, width), jnp.bfloat16)
    done = [pltpu.VMEM((size, rows, width), jnp.bfloat16)] if spread else []
    return pl.pallas_call(
        functools.partial(reduce_kernel, size, pairs, spread),
        out_shape=jax.ShapeDtypeStruct(
            (size, rows, width), jnp.bfloat16 if spread else jnp.float32
        ),
        in_specs=[VMEM],
        out_specs=VMEM,
        scratch_shapes=[kept] * 3
        + done
        + [pltpu.SemaphoreType.DMA((pairs, size))] * 4
        + [pltpu.SemaphoreType.DMA((size,))] * 2,
        compiler_params=pltpu.CompilerParams(collective_id=number, has_side_effects=True),
    )(blocks)


def local_pass(queries, key_rows, values, decay_factors, key_width, value_width):
    count_of_tokens = queries.shape[0]
    head_count = queries.shape[1] // key_width
    blocks = count_of_tokens // BLK
    lower = jnp.tril(jnp.ones((BLK, BLK), jnp.float32))

    def arrange(source, feature_channels):
        return (
            source.astype(jnp.float32)
            .reshape(blocks, BLK, head_count, feature_channels)
            .transpose(0, 2, 1, 3)
        )

    query_blocks = arrange(queries, key_width) * key_width ** (-0.5)
    key_blocks = arrange(key_rows, key_width)
    value_blocks = arrange(values, value_width)
    cumulative = jnp.einsum("ts,nhsd->nhtd", lower, arrange(decay_factors, key_width), precision=highest)
    block_end = cumulative[:, :, -1:, :]
    query_decayed = query_blocks * jnp.exp(cumulative)
    key_inverse = key_blocks * jnp.exp(-cumulative)
    key_to_end = key_blocks * jnp.exp(block_end - cumulative)
    scores = jnp.einsum("nhtd,nhsd->nhts", query_decayed, key_inverse, precision=highest) * lower
    inner = jnp.einsum("nhts,nhsv->nhtv", scores, value_blocks, precision=highest)
    added = jnp.einsum("nhsd,nhsv->nhdv", key_to_end, value_blocks, precision=highest)
    state = jnp.zeros((head_count, key_width, value_width), jnp.float32)
    states = []
    for n in range(blocks):
        states.append(state)
        state = jnp.exp(block_end[n, :, 0])[:, :, None] * state + added[n]
    ends = block_end[:, :, 0]
    return (query_decayed, inner, jnp.stack(states), ends, state)


def finish_pass(query_decayed, inner, states, ends, entering):
    before = jnp.cumsum(ends, axis=0) - ends
    states = states + jnp.exp(before)[:, :, :, None] * entering[None]
    out = inner + jnp.einsum("nhtd,nhdv->nhtv", query_decayed, states, precision=highest)
    blocks, heads, rows, width = out.shape
    return out.transpose(0, 2, 1, 3).reshape(blocks * rows, heads, width)


def entering_state(totals, states, index):
    size = totals.shape[0]
    k = jnp.arange(size)
    reached = (k < index)[:, None]
    masked = jnp.where(reached, totals, 0.0)
    after = (k[None, :] > k[:, None]).astype(jnp.float32)
    behind = jnp.sum(after[:, :, None] * masked[None], axis=1)
    factor = jnp.where(reached, jnp.exp(behind), 0.0)
    return jnp.sum(factor[:, :, None] * states.astype(jnp.float32), axis=0)


def head_norm(attention, head_gain, gate):
    inverse_rms = lax.rsqrt(jnp.mean(attention * attention, axis=-1, keepdims=True) + epsilon)
    gate_silu = jax.nn.silu(gate.astype(jnp.float32).reshape(attention.shape))
    mixed_rows = attention * inverse_rms * head_gain * gate_silu
    return mixed_rows.astype(jnp.bfloat16).reshape(attention.shape[0], -1)


def rms_scale(residual, gain_vector):
    as_float = residual.astype(jnp.float32)
    inverse_rms = lax.rsqrt(jnp.mean(as_float * as_float, axis=-1, keepdims=True) + epsilon)
    return (as_float * inverse_rms * gain_vector).astype(jnp.bfloat16)


def route_positions(block_routes, experts):
    flattened = block_routes.reshape(-1)
    amount = flattened.shape[0]
    onehot = flattened[:, None] == jnp.arange(experts, dtype=jnp.int32)[None, :]
    earlier = jnp.tril(jnp.ones((amount, amount), jnp.bfloat16), -1)
    before = jnp.dot(earlier, onehot.astype(jnp.bfloat16), preferred_element_type=jnp.float32)
    ranking = jnp.sum(jnp.where(onehot, before, 0.0), axis=1).astype(jnp.int32)
    return ranking.reshape(block_routes.shape)


def shards(
    query_first,
    key_first,
    value_first,
    decay_first,
    gate_first,
    norm_first,
    proj_first,
    query_second,
    key_second,
    value_second,
    decay_second,
    gate_second,
    norm_second,
    proj_second,
    residual_in,
    expert_norm,
    route_ids,
    route_weight,
    expert_gate,
    expert_up,
    expert_down,
):
    sp_size, tp_size = lax.axis_size("sp"), lax.axis_size("tp")
    sp_index, tp_index = lax.axis_index("sp"), lax.axis_index("tp")
    first = local_pass(query_first, key_first, value_first, decay_first, KA, VA)
    second = local_pass(query_second, key_second, value_second, decay_second, KB, VB)
    total_first = jnp.sum(first[3], axis=0).reshape(1, -1)
    total_second = jnp.sum(second[3], axis=0).reshape(1, -1)
    totals = jnp.concatenate((total_first, total_second), axis=1)
    totals = jnp.broadcast_to(totals, (8, totals.shape[1]))
    all_totals, all_first, all_second, *columns = exchange(
        (
            totals,
            first[4].reshape(-1, VA).astype(jnp.bfloat16),
            second[4].reshape(-1, VB).astype(jnp.bfloat16),
            proj_first,
            proj_second,
        ),
        "sp",
        sp_size,
        False,
        0,
    )
    columns = [part.transpose(1, 0, 2).reshape(part.shape[1], -1) for part in columns]
    projection = jnp.concatenate(columns, axis=0)
    cut = total_first.shape[1]
    enter_first = entering_state(all_totals[:, 0, :cut], all_first, sp_index)
    enter_second = entering_state(all_totals[:, 0, cut:], all_second, sp_index)
    attention_first = finish_pass(*first[:4], enter_first.reshape(first[4].shape))
    attention_second = finish_pass(*second[:4], enter_second.reshape(second[4].shape))
    mixed_first = head_norm(attention_first, norm_first, gate_first)
    mixed_second = head_norm(attention_second, norm_second, gate_second)
    mixed_rows = jnp.concatenate((mixed_first, mixed_second), axis=1)
    partial_terms = jnp.dot(mixed_rows, projection, preferred_element_type=jnp.float32)
    block_tokens, top_count = route_ids.shape
    model_width = partial_terms.shape[1]
    own_tokens = block_tokens // tp_size
    by_owner = (tp_size, PAIR, own_tokens // PAIR, model_width)
    mixture = reduce_tp(partial_terms.astype(jnp.bfloat16).reshape(by_owner), False, 1)
    mixture = mixture.reshape(own_tokens, model_width)
    residual = (residual_in.astype(jnp.float32) + mixture).astype(jnp.bfloat16)
    normed = rms_scale(residual, expert_norm)
    gathered = gather_tp(normed.reshape(by_owner[1:]), False, 2)
    gathered = gathered.reshape(block_tokens, model_width)

    experts = sp_size
    capacity = 2 * top_count * block_tokens // experts
    quarter = capacity // tp_size
    slots = experts * quarter
    place = route_positions(route_ids, experts) - tp_index * quarter
    local = jnp.where((place >= 0) & (place < quarter), route_ids * quarter + place, -1)
    numbers = jnp.arange(slots, dtype=jnp.int32)
    chosen, weights = (False, 0.0)
    for c in range(top_count):
        chosen = chosen | (numbers[:, None] == local[None, :, c])
        weights = weights + jnp.where(
            numbers[None, :] == local[:, c, None], route_weight[:, c, None], 0.0
        )
    outgoing = jnp.dot(
        chosen.astype(jnp.bfloat16), gathered, preferred_element_type=jnp.float32
    ).astype(jnp.bfloat16)
    incoming = gather_tp(outgoing.reshape(experts, quarter, model_width), True, 3)
    incoming = incoming.reshape(-1, model_width)
    gate_part = jnp.dot(incoming, expert_gate[0], preferred_element_type=jnp.float32)
    up_part = jnp.dot(incoming, expert_up[0], preferred_element_type=jnp.float32)
    hidden = (jax.nn.silu(gate_part) * up_part).astype(jnp.bfloat16)
    produced = jnp.dot(hidden, expert_down[0], preferred_element_type=jnp.float32)
    produced = produced.astype(jnp.bfloat16).reshape(tp_size, experts, quarter, model_width)
    returned = reduce_tp(produced, True, 4)
    returned = returned.reshape(slots, model_width)
    coarse = weights.astype(jnp.bfloat16)
    fine = (weights - coarse.astype(jnp.float32)).astype(jnp.bfloat16)
    weighted = jnp.dot(coarse, returned, preferred_element_type=jnp.float32)
    weighted = weighted + jnp.dot(fine, returned, preferred_element_type=jnp.float32)
    combined = reduce_tp(weighted.astype(jnp.bfloat16).reshape(by_owner), False, 5)
    combined = combined.reshape(own_tokens, model_width)
    return (residual.astype(jnp.float32) + combined).astype(jnp.bfloat16)


def solution(mesh):
    in_specs = (
        P("sp", "tp"),
        P("sp", "tp"),
        P("sp", "tp"),
        P("sp", "tp"),
        P("sp", "tp"),
        P(),
        P("tp", "sp"),
        P("sp", "tp"),
        P("sp", "tp"),
        P("sp", "tp"),
        P("sp", "tp"),
        P("sp", "tp"),
        P(),
        P("tp", "sp"),
        P(("sp", "tp"), None),
        P(),
        P("sp", None),
        P("sp", None),
        P("sp", None, "tp"),
        P("sp", None, "tp"),
        P("sp", "tp", None),
    )
    out_specs = P(("sp", "tp"), None)
    return jax.shard_map(shards, mesh=mesh, in_specs=in_specs, out_specs=out_specs, check_vma=False)
```

profile of v0, /device:TPU:1, one launch (start us, length us, event | category | flops | bytes accessed | tf_op | source)
XLA Modules:
  0.0 247.4 jit_solution(18302834398684022188)
XLA Ops:
  0.0 1.1 reshape.518
  1.2 0.4 convolution_bitcast_fusion
  1.6 1.0 reshape.536
  2.6 0.9 reshape.521
  3.5 0.4 fusion.47
  3.9 0.5 broadcast.264
  4.5 0.7 fusion.118
  5.6 0.7 fusion.98.refs_2_
  6.3 1.2 convolution_bitcast_fusion.1
  7.5 0.4 fusion.69
  8.0 0.8 fusion.97
  8.9 0.6 broadcast_in_dim.118.refs_0_
  9.5 55.3 %shard_map.199 = (f32[8,8,256]{2,1,0:T(8,128)}, bf16[8,128,256]{2,1,0:T(8,128)(2,1)}, bf16[8,128,128]{2,1,0:T(8,128)(2,1)}, bf16[8,256,256]{2,1,0:T(8,128)(2,1)}, bf16[8,256,256]{2,1,0:T(8,128)(2,1)}) custom-call(f32[8,256]{1,0:T(8,128)} %broadcast_in_dim.118.refs_0_, bf16[128,256]{1,0:T(8,128)(2,1)} %get-tuple-element.29.refs_1_, ...), custom_call_target="tpu_custom_call" | custom-call | tf_op jit(solution)/shard_map/pallas_call | solution.py:68
  64.8 0.9 copy.94
  65.7 0.8 slice.105
  66.7 1.2 multiply_reduce_fusion.1
  67.9 0.2 mul.388
  68.1 0.6 convolution_multiply_fusion
  68.8 0.3 fusion.73
  69.1 0.6 multiply_reduce_fusion.2
  69.8 0.3 mul.409
  70.2 0.2 copy.96
  70.4 1.3 multiply_reduce_fusion
  71.8 0.9 convert_multiply_fusion.7
  72.6 1.2 convolution_multiply_fusion.1
  73.8 0.3 fusion.143
  74.1 1.6 multiply_reduce_fusion.3
  75.8 0.7 broadcast_bitcast_fusion
  76.4 1.2 fusion.60
  77.6 1.5 copy.99
  79.2 0.5 copy.100
  79.7 3.0 %convolution_convert_fusion.1 = bf16[256,2048]{1,0:T(8,128)(2,1)} fusion(bf16[256,2048]{0,1:T(8,128)(2,1)S(1)} %bitcast.189, bf16[256,2048]{0,1:T(8,128)(2,1)} %bitcast.188, bf16[256,256]{1,0:T(8,128)(2,1)S(1)} %get-tuple-element.62, bf16[256,256]{1,0:T(8,128)(2,1)S(1)} %get-tuple-element.61), kind=kOutput, calls=%fused_computation.8 | convolution fusion | flops 542113792 | bytes 3407872 | tf_op jit(solution)/shard_map/dot_general | solution.py:367
  82.7 13.3 %shard_map.200 = f32[2,32,2048]{2,1,0:T(8,128)} custom-call(bf16[4,2,32,2048]{3,2,1,0:T(8,128)(2,1)} %bitcast.185), custom_call_target="tpu_custom_call" | custom-call | tf_op jit(solution)/shard_map/pallas_call | solution.py:223
  96.0 1.2 fusion.15
  97.3 0.8 fusion.17
  98.1 11.7 %shard_map.201 = bf16[4,2,32,2048]{3,2,1,0:T(8,128)(2,1)} custom-call(bf16[2,32,2048]{2,1,0:T(8,128)(2,1)} %bitcast.184), custom_call_target="tpu_custom_call" | custom-call | tf_op jit(solution)/shard_map/pallas_call | solution.py:146
  110.1 0.3 fusion.12
  110.8 0.2 slice_reduce_fusion.1
  111.0 2.6 %convolution_convert_fusion.2 = bf16[256,2048]{1,0:T(8,128)(2,1)} fusion(bf16[256,2048]{1,0:T(8,128)(2,1)} %bitcast.180, s32[256]{0:T(256)S(1)} %get-tuple-element.19, s32[256]{0:T(256)S(1)} %get-tuple-element.18), kind=kOutput, calls=%fused_computation.10 | convolution fusion | flops 269156352 | bytes 2099200 | tf_op jit(solution)/shard_map/dot_general | solution.py:392
  113.6 55.8 %shard_map.202 = bf16[4,8,32,2048]{3,2,1,0:T(8,128)(2,1)} custom-call(bf16[8,32,2048]{2,1,0:T(8,128)(2,1)} %bitcast.176), custom_call_target="tpu_custom_call" | custom-call | tf_op jit(solution)/shard_map/pallas_call | solution.py:146
  169.4 7.5 %fusion.1 = f32[1024,896]{1,0:T(8,128)S(1)} fusion(bf16[1024,2048]{1,0:T(8,128)(2,1)} %bitcast.177, bf16[1,2048,896]{2,1,0:T(8,128)(2,1)} %param.40), kind=kOutput, calls=%fused_computation.2 | convolution fusion | flops 3758096384 | bytes 11534336 | tf_op jit(solution)/shard_map/dot_general | solution.py:398
  177.0 4.8 %multiply_convert_fusion = bf16[1024,896]{1,0:T(8,128)(2,1)S(1)} fusion(f32[1024,896]{1,0:T(8,128)S(1)} %fusion.1, bf16[1024,2048]{1,0:T(8,128)(2,1)S(1)} %bitcast.178, bf16[1,2048,896]{2,1,0:T(8,128)(2,1)S(1)} %copy-done.13), kind=kOutput, calls=%fused_computation.6 | convolution fusion | flops 3763601408 | bytes 13369344 | tf_op jit(solution)/shard_map/dot_general | solution.py:397
  181.7 6.1 %convolution_convert_fusion = bf16[1024,2048]{1,0:T(8,128)(2,1)} fusion(bf16[1024,896]{1,0:T(8,128)(2,1)S(1)} %multiply_convert_fusion, bf16[1,896,2048]{2,1,0:T(8,128)(2,1)S(1)} %copy-done.14), kind=kOutput, calls=%fused_computation | convolution fusion | flops 3760193536 | bytes 9699328 | tf_op jit(solution)/shard_map/dot_general | solution.py:400
  187.8 42.3 %shard_map.203 = bf16[8,32,2048]{2,1,0:T(8,128)(2,1)} custom-call(bf16[4,8,32,2048]{3,2,1,0:T(8,128)(2,1)} %bitcast.179), custom_call_target="tpu_custom_call" | custom-call | tf_op jit(solution)/shard_map/pallas_call | solution.py:223
  230.1 1.8 fusion.93
  232.0 1.5 fusion.5
  233.5 12.1 %shard_map.204 = f32[2,32,2048]{2,1,0:T(8,128)} custom-call(bf16[4,2,32,2048]{3,2,1,0:T(8,128)(2,1)} %bitcast.181), custom_call_target="tpu_custom_call" | custom-call | tf_op jit(solution)/shard_map/pallas_call | solution.py:223
  245.6 1.8 fusion.18
  (65 shorter events, 1.8 us)
Async XLA Ops:
  0.0 7.5 %copy-start = (bf16[256,256]{1,0:T(8,128)(2,1)S(1)}, bf16[256,256]{1,0:T(8,128)(2,1)}, u32[]{:S(2)}) copy-start(bf16[256,256]{1,0:T(8,128)(2,1)} %param.23) | copy-start | bytes 393220
  0.0 7.5 %copy-start.7 = (bf16[256,128]{1,0:T(8,128)(2,1)S(1)}, bf16[256,128]{1,0:T(8,128)(2,1)}, u32[]{:S(2)}) copy-start(bf16[256,128]{1,0:T(8,128)(2,1)} %param.22) | copy-start | bytes 196612
  0.0 67.9 %copy-start.8 = (bf16[256,128]{1,0:T(8,128)(2,1)S(1)}, bf16[256,128]{1,0:T(8,128)(2,1)}, u32[]{:S(2)}) copy-start(bf16[256,128]{1,0:T(8,128)(2,1)} %param.28) | copy-start | bytes 196612
  68.1 0.6 copy-start.5
  68.1 8.3 %copy-start.12 = (f32[256]{0:T(256)S(1)}, f32[256]{0:T(256)}, u32[]{:S(2)}) copy-start(f32[256]{0:T(256)} %param.26) | copy-start | bytes 3076
  69.0 8.6 %copy-start.4 = (bf16[8,256,256]{2,1,0:T(8,128)(2,1)S(1)}, bf16[8,256,256]{2,1,0:T(8,128)(2,1)}, u32[]{:S(2)}) copy-start(bf16[8,256,256]{2,1,0:T(8,128)(2,1)} %get-tuple-element.13) | copy-start | bytes 3145732
  70.1 9.0 %copy-start.3 = (bf16[8,256,256]{2,1,0:T(8,128)(2,1)S(1)}, bf16[8,256,256]{2,1,0:T(8,128)(2,1)}, u32[]{:S(2)}) copy-start(bf16[8,256,256]{2,1,0:T(8,128)(2,1)} %get-tuple-element.14) | copy-start | bytes 3145732
  79.7 16.3 %copy-start.6 = (bf16[64,2048]{1,0:T(8,128)(2,1)S(1)}, bf16[64,2048]{1,0:T(8,128)(2,1)}, u32[]{:S(2)}) copy-start(bf16[64,2048]{1,0:T(8,128)(2,1)} %param.35) | copy-start | bytes 786436
  79.7 17.6 %copy-start.9 = (f32[2048]{0:T(1024)S(1)}, f32[2048]{0:T(1024)}, u32[]{:S(2)}) copy-start(f32[2048]{0:T(1024)} %param.36) | copy-start | bytes 24580
  79.7 30.1 %copy-start.10 = (s32[256,2]{0,1:T(2,128)S(1)}, s32[256,2]{0,1:T(2,128)}, u32[]{:S(2)}) copy-start(s32[256,2]{0,1:T(2,128)} %param.37) | copy-start | bytes 6148
  169.4 7.5 %copy-start.2 = (bf16[4,8,32,2048]{3,2,1,0:T(8,128)(2,1)S(1)}, bf16[4,8,32,2048]{3,2,1,0:T(8,128)(2,1)}, u32[]{:S(2)}) copy-start(bf16[4,8,32,2048]{3,2,1,0:T(8,128)(2,1)} %shard_map.202) | copy-start | bytes 12582916
  169.4 7.5 %copy-start.13 = (bf16[1,2048,896]{2,1,0:T(8,128)(2,1)S(1)}, bf16[1,2048,896]{2,1,0:T(8,128)(2,1)}, u32[]{:S(2)}) copy-start(bf16[1,2048,896]{2,1,0:T(8,128)(2,1)} %param.39) | copy-start | bytes 11010052
  177.0 4.8 %copy-start.14 = (bf16[1,896,2048]{2,1,0:T(8,128)(2,1)S(1)}, bf16[1,896,2048]{2,1,0:T(8,128)(2,1)}, u32[]{:S(2)}) copy-start(bf16[1,896,2048]{2,1,0:T(8,128)(2,1)} %param.41) | copy-start | bytes 11010052
  187.8 42.3 %copy-start.11 = (f32[256,2]{0,1:T(2,128)S(1)}, f32[256,2]{0,1:T(2,128)}, u32[]{:S(2)}) copy-start(f32[256,2]{0,1:T(2,128)} %param.38) | copy-start | bytes 6148
  230.1 1.9 copy-start.1
where the time goes:
time: 249 us; the launch traced here: 247 us
  Pallas kernels  190 us (76%)
  matrix products  34.5 us (14%)
  other arithmetic  11.2 us (4%)
  local copies, waits for them, and re-layouts  10.7 us (4%)
    pallas_call x3, Pallas kernels, reduce_tp(): pl.pallas_call(functools.partial(reduce_kernel, size, pairs, spread), out...  67.7 us
    pallas_call x2, Pallas kernels, gather_tp(): pl.pallas_call(functools.partial(gather_kernel, size, pairs, spread), out...  67.4 us
    pallas_call x1, Pallas kernels, exchange(): pl.pallas_call(functools.partial(exchange_kernel, axis, span, spread, cou...  55.3 us
    dot_general x1, matrix products, shards(): jnp.dot(incoming, expert_up[0], preferred_element_type=jnp.float32)  7.5 us
    dot_general x1, matrix products, shards(): jnp.dot(hidden, expert_down[0], preferred_element_type=jnp.float32)  6.05 us

commit v1 on v0

--- a/solution.py
+++ b/solution.py
@@ -94,64 +94,6 @@
         device_id=device,
         device_id_type=MESH,
     )
-
-
-def gather_kernel(size, pairs, spread, source, target, *sems):
-    sp_sems, pair_sems, far_sems = sems[:2], sems[2:4], sems[4:]
-    me, mine = lax.axis_index("sp"), lax.axis_index("tp")
-    sibling = {"tp": tp_member(0, True)}
-    far = [{"tp": tp_member(across, False)} for across in range(1, pairs)]
-    peers = [group_member("sp", size, step) for step in range(1, size)] if spread else []
-    greet([peer[2] for peer in peers] + [sibling] + far)
-    copies = []
-    for step, (_, other, device) in enumerate(peers, 1):
-        copies.append(remote(source.at[other], target.at[mine, me], sp_sems, step, device))
-        copies[-1].start()
-    passed, distant = [], []
-    for step in range(size):
-        if spread:
-            origin = lax.rem(me - step + size, size)
-        else:
-            origin = step
-        own = step == 0 or not spread
-        if not own:
-            copies[step - 1].wait_recv()
-        block = source.at[origin] if own else target.at[mine, origin]
-        for across in range(1, pairs):
-            copy = remote(
-                block, target.at[mine, origin], far_sems, (across, step), far[across - 1]
-            )
-            copy.start()
-            distant.append((copy, tp_member(pairs - across, False), origin, across, step))
-        copy = remote(block, target.at[mine, origin], pair_sems, (0, step), sibling)
-        copy.start()
-        passed.append(copy)
-        if own:
-            target[mine, origin] = source[origin]
-    for copy, sender, origin, across, step in distant:
-        copy.wait_recv()
-        block = target.at[sender, origin]
-        again = remote(block, block, pair_sems, (across, step), sibling)
-        again.start()
-        passed.append(again)
-    for copy in copies + [item[0] for item in distant]:
-        copy.wait_send()
-    for copy in passed:
-        copy.wait()
-
-
-def gather_tp(blocks, spread, number):
-    size, tp = blocks.shape[0], lax.axis_size("tp")
-    pairs = tp // PAIR
-    return pl.pallas_call(
-        functools.partial(gather_kernel, size, pairs, spread),
-        out_shape=jax.ShapeDtypeStruct((tp,) + blocks.shape, blocks.dtype),
-        in_specs=[VMEM],
-        out_specs=VMEM,
-        scratch_shapes=[pltpu.SemaphoreType.DMA((size,))] * 2
-        + [pltpu.SemaphoreType.DMA((pairs, size))] * 4,
-        compiler_params=pltpu.CompilerParams(collective_id=number, has_side_effects=True),
-    )(blocks)
 
 
 def reduce_kernel(size, pairs, spread, source, target, near, paired, arrived, *rest):
@@ -235,6 +177,329 @@
     )(blocks)
 
 
+def ring_offset(step, lines):
+    return lax.rem(step * (lines // 2), lines) + step // 2
+
+
+def experts_kernel(
+    size,
+    tp,
+    slots_across,
+    slots_down,
+    route_weight,
+    residual,
+    gain,
+    gate_hbm,
+    up_hbm,
+    down_hbm,
+    out,
+    gate_weights,
+    up_weights,
+    down_weights,
+    chosen_rows,
+    rows,
+    normed,
+    hidden,
+    pieces,
+    near,
+    paired,
+    arrived,
+    done,
+    returned,
+    total,
+    columns,
+    collected,
+    load_sems,
+    *sems,
+):
+    out_sems, far_sems, pair_sems, near_sems, cross_sems, back_sems, last_sems = (
+        sems[2 * i : 2 * i + 2] for i in range(7)
+    )
+    pairs = tp // PAIR
+    lines = size // PAIR
+    capacity, width = rows.shape[2:]
+    tokens = residual.shape[0]
+    me, mine = lax.axis_index("sp"), lax.axis_index("tp")
+    line, seat = me // PAIR, lax.rem(me, PAIR)
+    sibling = {"tp": tp_member(0, True)}
+
+    def forth(k):
+        across = lax.rem(line + ring_offset(k // PAIR, lines), lines)
+        return across * PAIR + lax.rem(seat + lax.rem(k, PAIR), PAIR)
+
+    def back(k):
+        across = lax.rem(line - ring_offset(k // PAIR, lines) + lines, lines)
+        return across * PAIR + lax.rem(seat + lax.rem(k, PAIR), PAIR)
+
+    loads = [
+        pltpu.make_async_copy(gate_hbm, gate_weights, load_sems.at[0]),
+        pltpu.make_async_copy(up_hbm, up_weights, load_sems.at[1]),
+        pltpu.make_async_copy(down_hbm, down_weights, load_sems.at[2]),
+    ]
+    for load in loads:
+        load.start()
+    peers = [group_member("sp", size, step)[2] for step in range(1, size)]
+    peers += [group_member("tp", tp, step)[2] for step in range(1, tp)]
+    greet(peers)
+
+    def outward(k):
+        return remote(
+            chosen_rows.at[k], rows.at[me, mine], out_sems, k, {"sp": forth(k)}
+        )
+
+    def choose(k, target, *index):
+        numbers = lax.broadcasted_iota(jnp.int32, (capacity, tokens), 0) + forth(k) * capacity
+        chosen = numbers == slots_across[0:1, :]
+        for c in range(1, slots_across.shape[0]):
+            chosen = chosen | (numbers == slots_across[c : c + 1, :])
+        picked = jnp.where(chosen, 1.0, 0.0).astype(jnp.bfloat16)
+        picked = jnp.dot(picked, residual[...], preferred_element_type=jnp.float32)
+        target[index] = picked.astype(jnp.bfloat16)
+
+    choose(0, rows, me, mine)
+
+    def send_step(k, carry):
+        choose(k, chosen_rows, k)
+        outward(k).start()
+        return carry
+
+    lax.fori_loop(1, size, send_step, 0)
+
+    def to_far(k, across):
+        block = rows.at[back(k), mine]
+        return remote(block, block, far_sems, (across, k), {"tp": tp_member(across, False)})
+
+    def to_pair(k, across):
+        origin = tp_member(pairs - across, False) if across else mine
+        block = rows.at[back(k), origin]
+        return remote(block, block, pair_sems, (across, k), sibling)
+
+    def forward(k):
+        for across in range(1, pairs):
+            to_far(k, across).start()
+        to_pair(k, 0).start()
+
+    def forward_group(g):
+        for j in range(PAIR):
+            k = g * PAIR + j
+            outward(k).wait_recv()
+            forward(k)
+
+    def collect_group(g):
+        for j in range(PAIR):
+            for across in range(1, pairs):
+                to_far(g * PAIR + j, across).wait_recv()
+                to_pair(g * PAIR + j, across).start()
+        for j in range(PAIR):
+            for across in range(pairs):
+                to_pair(g * PAIR + j, across).wait_recv()
+
+    def to_near(g, across):
+        return remote(
+            pieces.at[g, tp_member(across, True)],
+            near.at[g, across],
+            near_sems,
+            (across, g),
+            sibling,
+        )
+
+    def to_cross(g, across):
+        return remote(
+            paired.at[g, across],
+            arrived.at[g, across],
+            cross_sems,
+            (across, g),
+            {"tp": tp_member(across, False)},
+        )
+
+    def homeward(k):
+        return remote(
+            done.at[k], returned.at[me], back_sems, k, {"sp": back(k)}
+        )
+
+    def run_group(g):
+        for j in range(PAIR):
+            origin = back(g * PAIR + j)
+            block = jnp.concatenate([rows[origin, t] for t in range(tp)], axis=1)
+            block = block.astype(jnp.float32)
+            inverse = lax.rsqrt(jnp.mean(block * block, axis=1, keepdims=True) + epsilon)
+            normed[j * capacity : (j + 1) * capacity] = (block * inverse * gain[...]).astype(
+                jnp.bfloat16
+            )
+        gate_part = jnp.dot(normed[...], gate_weights[...], preferred_element_type=jnp.float32)
+        up_part = jnp.dot(normed[...], up_weights[...], preferred_element_type=jnp.float32)
+        hidden[...] = (jax.nn.silu(gate_part) * up_part).astype(jnp.bfloat16)
+        for t in range(tp):
+            piece = jnp.dot(
+                hidden[...],
+                down_weights[:, t * width : (t + 1) * width],
+                preferred_element_type=jnp.float32,
+            )
+            pieces[g, t] = piece.astype(jnp.bfloat16)
+        for across in list(range(1, pairs)) + [0]:
+            to_near(g, across).start()
+
+    def pair_sum(g, across):
+        own = pieces[g, tp_member(across, False)].astype(jnp.float32)
+        return own + near[g, across].astype(jnp.float32)
+
+    def cross_group(g):
+        for across in range(1, pairs):
+            to_near(g, across).wait_recv()
+            paired[g, across] = pair_sum(g, across).astype(jnp.bfloat16)
+            to_cross(g, across).start()
+
+    def finish_group(g, first):
+        to_near(g, 0).wait_recv()
+        summed = pair_sum(g, 0)
+        for across in range(1, pairs):
+            to_cross(g, across).wait_recv()
+            summed = summed + arrived[g, across].astype(jnp.float32)
+        summed = summed.astype(jnp.bfloat16)
+        for j in range(PAIR):
+            part = summed[j * capacity : (j + 1) * capacity]
+            if first and j == 0:
+                returned[me] = part
+            else:
+                done[g * PAIR + j] = part
+                homeward(g * PAIR + j).start()
+
+    forward(0)
+    outward(1).wait_recv()
+    forward(1)
+    for load in loads:
+        load.wait()
+    groups = size // PAIR
+
+    def group_step(g, carry):
+        @pl.when(g + 1 < groups)
+        def _():
+            forward_group(g + 1)
+
+        collect_group(g)
+        run_group(g)
+
+        @pl.when(g == 1)
+        def _():
+            finish_group(0, True)
+
+        @pl.when(g > 1)
+        def _():
+            finish_group(g - 1, False)
+
+        cross_group(g)
+        return carry
+
+    lax.fori_loop(0, groups, group_step, 0)
+    finish_group(groups - 1, groups == 1)
+
+    def combine(k):
+        expert = forth(k)
+        numbers = lax.broadcasted_iota(jnp.int32, (tokens, capacity), 1) + expert * capacity
+        weights = jnp.zeros((tokens, capacity), jnp.float32)
+        for c in range(route_weight.shape[1]):
+            weights = weights + jnp.where(
+                numbers == slots_down[:, c : c + 1], route_weight[:, c : c + 1], 0.0
+            )
+        coarse = weights.astype(jnp.bfloat16)
+        fine = (weights - coarse.astype(jnp.float32)).astype(jnp.bfloat16)
+        part = jnp.dot(coarse, returned[expert], preferred_element_type=jnp.float32)
+        return part + jnp.dot(fine, returned[expert], preferred_element_type=jnp.float32)
+
+    total[...] = residual[...].astype(jnp.float32) + combine(0)
+
+    def combine_step(k, carry):
+        homeward(k).wait_recv()
+        total[...] += combine(k)
+        return carry
+
+    lax.fori_loop(1, size, combine_step, 0)
+    own = tokens // tp
+    for t in range(tp):
+        columns[t] = total[t * own : (t + 1) * own].astype(jnp.bfloat16)
+
+    def to_owner(step):
+        _, other, device = group_member("tp", tp, step)
+        return remote(columns.at[other], collected.at[mine], last_sems, step, device)
+
+    for step in range(1, tp):
+        to_owner(step).start()
+    collected[mine] = columns[mine]
+    for step in range(1, tp):
+        to_owner(step).wait_recv()
+    for t in range(tp):
+        out[:, t * width : (t + 1) * width] = collected[t]
+
+    def drain_step(k, carry):
+        outward(k).wait_send()
+        homeward(k).wait_send()
+        return carry
+
+    lax.fori_loop(1, size, drain_step, 0)
+
+    def drain_pair(k, carry):
+        for across in range(pairs):
+            to_pair(k, across).wait_send()
+            if across:
+                to_far(k, across).wait_send()
+        return carry
+
+    lax.fori_loop(0, size, drain_pair, 0)
+
+    def drain_group(g, carry):
+        for across in range(pairs):
+            to_near(g, across).wait_send()
+            if across:
+                to_cross(g, across).wait_send()
+        return carry
+
+    lax.fori_loop(0, groups, drain_group, 0)
+    for step in range(1, tp):
+        to_owner(step).wait_send()
+
+
+def run_experts(slots, route_weight, residual, gain, gate, up, down, capacity, number):
+    size, tp = lax.axis_size("sp"), lax.axis_size("tp")
+    pairs, groups = tp // PAIR, size // PAIR
+    tokens, width = residual.shape
+    model, hidden = gate.shape
+    half = jnp.bfloat16
+    taken = PAIR * capacity
+    anywhere = pl.BlockSpec(memory_space=pl.ANY)
+    dma = pltpu.SemaphoreType.DMA
+    return pl.pallas_call(
+        functools.partial(experts_kernel, size, tp),
+        out_shape=jax.ShapeDtypeStruct((tokens // tp, model), half),
+        in_specs=[VMEM] * 5 + [anywhere] * 3,
+        out_specs=VMEM,
+        scratch_shapes=[
+            pltpu.VMEM(gate.shape, half),
+            pltpu.VMEM(up.shape, half),
+            pltpu.VMEM(down.shape, half),
+            pltpu.VMEM((size, capacity, width), half),
+            pltpu.VMEM((size, tp, capacity, width), half),
+            pltpu.VMEM((taken, model), half),
+            pltpu.VMEM((taken, hidden), half),
+            pltpu.VMEM((groups, tp, taken, width), half),
+            pltpu.VMEM((groups, pairs, taken, width), half),
+            pltpu.VMEM((groups, pairs, taken, width), half),
+            pltpu.VMEM((groups, pairs, taken, width), half),
+            pltpu.VMEM((size, capacity, width), half),
+            pltpu.VMEM((size, capacity, width), half),
+            pltpu.VMEM((tokens, width), jnp.float32),
+            pltpu.VMEM((tp, tokens // tp, width), half),
+            pltpu.VMEM((tp, tokens // tp, width), half),
+            dma((3,)),
+        ]
+        + [dma((size,))] * 2
+        + [dma((pairs, size))] * 4
+        + [dma((pairs, groups))] * 4
+        + [dma((size,))] * 2
+        + [dma((tp,))] * 2,
+        compiler_params=pltpu.CompilerParams(collective_id=number, has_side_effects=True),
+    )(slots.T, slots, route_weight, residual, gain, gate, up, down)
+
+
 def local_pass(queries, key_rows, values, decay_factors, key_width, value_width):
     count_of_tokens = queries.shape[0]
     head_count = queries.shape[1] // key_width
@@ -292,12 +557,6 @@
     gate_silu = jax.nn.silu(gate.astype(jnp.float32).reshape(attention.shape))
     mixed_rows = attention * inverse_rms * head_gain * gate_silu
     return mixed_rows.astype(jnp.bfloat16).reshape(attention.shape[0], -1)
-
-
-def rms_scale(residual, gain_vector):
-    as_float = residual.astype(jnp.float32)
-    inverse_rms = lax.rsqrt(jnp.mean(as_float * as_float, axis=-1, keepdims=True) + epsilon)
-    return (as_float * inverse_rms * gain_vector).astype(jnp.bfloat16)
 
 
 def route_positions(block_routes, experts):
@@ -334,7 +593,7 @@
     expert_down,
 ):
     sp_size, tp_size = lax.axis_size("sp"), lax.axis_size("tp")
-    sp_index, tp_index = lax.axis_index("sp"), lax.axis_index("tp")
+    sp_index = lax.axis_index("sp")
     first = local_pass(query_first, key_first, value_first, decay_first, KA, VA)
     second = local_pass(query_second, key_second, value_second, decay_second, KB, VB)
     total_first = jnp.sum(first[3], axis=0).reshape(1, -1)
@@ -368,46 +627,31 @@
     block_tokens, top_count = route_ids.shape
     model_width = partial_terms.shape[1]
     own_tokens = block_tokens // tp_size
-    by_owner = (tp_size, PAIR, own_tokens // PAIR, model_width)
-    mixture = reduce_tp(partial_terms.astype(jnp.bfloat16).reshape(by_owner), False, 1)
-    mixture = mixture.reshape(own_tokens, model_width)
-    residual = (residual_in.astype(jnp.float32) + mixture).astype(jnp.bfloat16)
-    normed = rms_scale(residual, expert_norm)
-    gathered = gather_tp(normed.reshape(by_owner[1:]), False, 2)
-    gathered = gathered.reshape(block_tokens, model_width)
+    own_columns = model_width // tp_size
+    by_owner = (block_tokens, tp_size, own_columns)
+    partial_terms = partial_terms.astype(jnp.bfloat16).reshape(by_owner).transpose(1, 0, 2)
+    partial_terms = partial_terms.reshape(tp_size, PAIR, block_tokens // PAIR, own_columns)
+    mixture = reduce_tp(partial_terms, False, 1).reshape(block_tokens, own_columns)
+    own_tokens = residual_in.shape[0]
+    residual = residual_in.reshape(own_tokens, tp_size, own_columns).transpose(1, 0, 2)
+    (residual,) = exchange((residual,), "tp", tp_size, True, 2)
+    residual = residual.reshape(block_tokens, own_columns)
+    residual = (residual.astype(jnp.float32) + mixture).astype(jnp.bfloat16)
 
     experts = sp_size
     capacity = 2 * top_count * block_tokens // experts
-    quarter = capacity // tp_size
-    slots = experts * quarter
-    place = route_positions(route_ids, experts) - tp_index * quarter
-    local = jnp.where((place >= 0) & (place < quarter), route_ids * quarter + place, -1)
-    numbers = jnp.arange(slots, dtype=jnp.int32)
-    chosen, weights = (False, 0.0)
-    for c in range(top_count):
-        chosen = chosen | (numbers[:, None] == local[None, :, c])
-        weights = weights + jnp.where(
-            numbers[None, :] == local[:, c, None], route_weight[:, c, None], 0.0
-        )
-    outgoing = jnp.dot(
-        chosen.astype(jnp.bfloat16), gathered, preferred_element_type=jnp.float32
-    ).astype(jnp.bfloat16)
-    incoming = gather_tp(outgoing.reshape(experts, quarter, model_width), True, 3)
-    incoming = incoming.reshape(-1, model_width)
-    gate_part = jnp.dot(incoming, expert_gate[0], preferred_element_type=jnp.float32)
-    up_part = jnp.dot(incoming, expert_up[0], preferred_element_type=jnp.float32)
-    hidden = (jax.nn.silu(gate_part) * up_part).astype(jnp.bfloat16)
-    produced = jnp.dot(hidden, expert_down[0], preferred_element_type=jnp.float32)
-    produced = produced.astype(jnp.bfloat16).reshape(tp_size, experts, quarter, model_width)
-    returned = reduce_tp(produced, True, 4)
-    returned = returned.reshape(slots, model_width)
-    coarse = weights.astype(jnp.bfloat16)
-    fine = (weights - coarse.astype(jnp.float32)).astype(jnp.bfloat16)
-    weighted = jnp.dot(coarse, returned, preferred_element_type=jnp.float32)
-    weighted = weighted + jnp.dot(fine, returned, preferred_element_type=jnp.float32)
-    combined = reduce_tp(weighted.astype(jnp.bfloat16).reshape(by_owner), False, 5)
-    combined = combined.reshape(own_tokens, model_width)
-    return (residual.astype(jnp.float32) + combined).astype(jnp.bfloat16)
+    slots = route_ids * capacity + route_positions(route_ids, experts)
+    return run_experts(
+        slots,
+        route_weight,
+        residual,
+        expert_norm.reshape(1, -1),
+        expert_gate[0],
+        expert_up[0],
+        expert_down[0],
+        capacity,
+        3,
+    )
 
 
 def solution(mesh):

time: 249 us -> 207 us (0.83)
  matrix products: 34.5 us -> 9.2 us
  Pallas kernels: 190 us -> 170 us
  local copies, waits for them, and re-layouts: 10.7 us -> 15.4 us
    pallas_call x3 -> x1, Pallas kernels: 67.7 us -> 13.3 us  [reduce_tp(): pl.pallas_call(functools.partial(reduce_kernel, size, pairs, spread), out...]
    pallas_call x2 -> x1, Pallas kernels: 67.4 us -> 93.8 us  [run_experts(): pl.pallas_call(functools.partial(experts_kernel, size, tp), out_shape=jax...]
    dot_general x6 -> x0, matrix products: 24.3 us -> none  [the longest x1 7.5 us: shards(): jnp.dot(incoming, expert_up[0], preferred_element_type=jnp.float32)]
    pallas_call x1 -> x2, Pallas kernels: 55.3 us -> 62.7 us  [exchange(): pl.pallas_call(functools.partial(exchange_kernel, axis, span, spread, cou...]
where the time goes in v1:
time: 207 us; the launch traced here: 205 us
  Pallas kernels  170 us (82%)
  local copies, waits for them, and re-layouts  15.4 us (7%)
  other arithmetic  9.79 us (5%)
  matrix products  9.2 us (4%)
    pallas_call x1, Pallas kernels, run_experts(): pl.pallas_call(functools.partial(experts_kernel, size, tp), out_shape=jax...  93.8 us
    pallas_call x2, Pallas kernels, exchange(): pl.pallas_call(functools.partial(exchange_kernel, axis, span, spread, cou...  62.7 us
    pallas_call x1, Pallas kernels, reduce_tp(): pl.pallas_call(functools.partial(reduce_kernel, size, pairs, spread), out...  13.3 us

profile of v1, /device:TPU:1, one launch (start us, length us, event | category | flops | bytes accessed | tf_op | source)
XLA Modules:
  0.0 204.6 jit_solution(12228660051086770171)
XLA Ops:
  0.0 1.1 reshape.494
  1.2 0.4 convolution_bitcast_fusion
  1.6 1.0 reshape.507
  2.6 0.9 reshape.497
  3.5 0.4 fusion.35
  3.9 0.5 broadcast.241
  4.5 0.7 fusion.93
  5.1 0.1 multiply_add_fusion
  5.6 0.7 fusion.73.refs_2_
  6.3 1.2 convolution_bitcast_fusion.1
  7.5 0.4 fusion.54
  8.0 0.8 fusion.72
  8.9 0.6 broadcast_in_dim.89.refs_0_
  9.4 55.3 %shard_map.200 = (f32[8,8,256]{2,1,0:T(8,128)}, bf16[8,128,256]{2,1,0:T(8,128)(2,1)}, bf16[8,128,128]{2,1,0:T(8,128)(2,1)}, bf16[8,256,256]{2,1,0:T(8,128)(2,1)}, bf16[8,256,256]{2,1,0:T(8,128)(2,1)}) custom-call(f32[8,256]{1,0:T(8,128)} %broadcast_in_dim.89.refs_0_, bf16[128,256]{1,0:T(8,128)(2,1)} %get-tuple-element.25.refs_1_, ...), custom_call_target="tpu_custom_call" | custom-call | tf_op jit(solution)/shard_map/pallas_call | solution.py:68
  64.8 0.9 copy.106
  65.7 0.8 slice.91
  66.7 1.2 multiply_reduce_fusion.1
  67.9 0.2 mul.364
  68.1 0.6 convolution_multiply_fusion
  68.7 0.3 fusion.58
  69.0 0.6 multiply_reduce_fusion.2
  69.6 0.1 copy.118
  69.8 0.3 mul.385
  70.1 0.2 copy.108
  70.3 2.0 multiply_reduce_fusion
  72.3 0.9 convert_multiply_fusion.5
  73.2 1.2 convolution_multiply_fusion.1
  74.4 0.2 fusion.114
  74.7 1.6 multiply_reduce_fusion.3
  76.4 0.7 broadcast_bitcast_fusion
  77.0 1.2 fusion.47
  78.2 1.5 copy.111
  79.7 0.5 copy.112
  80.3 2.0 convolution_convert_fusion
  82.3 1.1 copy.161
  83.4 13.3 %shard_map.201 = f32[2,128,512]{2,1,0:T(8,128)} custom-call(bf16[4,2,128,512]{3,2,1,0:T(8,128)(2,1)} %bitcast.164), custom_call_target="tpu_custom_call" | custom-call | tf_op jit(solution)/shard_map/pallas_call | solution.py:165
  96.7 0.7 copy.162
  97.4 7.4 %shard_map.199 = bf16[4,64,512]{2,1,0:T(8,128)(2,1)} custom-call(bf16[4,64,512]{2,1,0:T(8,128)(2,1)} %bitcast.176), custom_call_target="tpu_custom_call" | custom-call | tf_op jit(solution)/shard_map/pallas_call | solution.py:68
  104.8 1.9 fusion.13.residual
  106.7 0.1 copy.99
  106.8 0.1 eq.15
  107.0 0.3 fusion.4
  107.4 0.1 convert_element_type.69
  107.5 0.1 copy.100
  107.7 0.7 copy.114.slots_across
  108.4 0.8 copy.115.route_weight
  109.2 93.8 %shard_map.202 = bf16[64,2048]{1,0:T(8,128)(2,1)} custom-call(s32[2,256]{1,0:T(2,128)} %copy.114.slots_across, s32[256,2]{1,0:T(8,128)} %copy-done.1, f32[256,2]{1,0:T(8,128)} %copy.115.route_weight, bf16[256,512]{1,0:T(8,128)(2,1)} %fusion.13.residual, f32[1,2048]{1,0:T(1,128)} %bitcast.191, bf16[2048,896]{1,0:T(8,128)(2,1)} %bitcast.165, ...), custom_call_target="tpu_custom_call" | custom-call | tf_op jit(solution)/shard_map/pallas_call | solution.py:470
  203.0 1.7 copy.164
  (49 shorter events, 1.0 us)
Async XLA Ops:
  0.0 7.5 %copy-start = (bf16[256,256]{1,0:T(8,128)(2,1)S(1)}, bf16[256,256]{1,0:T(8,128)(2,1)}, u32[]{:S(2)}) copy-start(bf16[256,256]{1,0:T(8,128)(2,1)} %param.23) | copy-start | bytes 393220
  0.0 7.5 %copy-start.6 = (bf16[256,128]{1,0:T(8,128)(2,1)S(1)}, bf16[256,128]{1,0:T(8,128)(2,1)}, u32[]{:S(2)}) copy-start(bf16[256,128]{1,0:T(8,128)(2,1)} %param.22) | copy-start | bytes 196612
  0.0 67.8 %copy-start.7 = (bf16[256,128]{1,0:T(8,128)(2,1)S(1)}, bf16[256,128]{1,0:T(8,128)(2,1)}, u32[]{:S(2)}) copy-start(bf16[256,128]{1,0:T(8,128)(2,1)} %param.28) | copy-start | bytes 196612
  68.1 1.7 copy-start.4
  68.1 8.9 %copy-start.10 = (f32[256]{0:T(256)S(1)}, f32[256]{0:T(256)}, u32[]{:S(2)}) copy-start(f32[256]{0:T(256)} %param.26) | copy-start | bytes 3076
  69.0 9.2 %copy-start.3 = (bf16[8,256,256]{2,1,0:T(8,128)(2,1)S(1)}, bf16[8,256,256]{2,1,0:T(8,128)(2,1)}, u32[]{:S(2)}) copy-start(bf16[8,256,256]{2,1,0:T(8,128)(2,1)} %get-tuple-element.13) | copy-start | bytes 3145732
  70.1 9.6 %copy-start.2 = (bf16[8,256,256]{2,1,0:T(8,128)(2,1)S(1)}, bf16[8,256,256]{2,1,0:T(8,128)(2,1)}, u32[]{:S(2)}) copy-start(bf16[8,256,256]{2,1,0:T(8,128)(2,1)} %get-tuple-element.14) | copy-start | bytes 3145732
  80.3 16.5 %copy-start.5 = (bf16[64,2048]{1,0:T(8,128)(2,1)S(1)}, bf16[64,2048]{1,0:T(8,128)(2,1)}, u32[]{:S(2)}) copy-start(bf16[64,2048]{1,0:T(8,128)(2,1)} %param.35) | copy-start | bytes 786436
  82.3 24.4 %copy-start.8 = (s32[256,2]{0,1:T(2,128)S(1)}, s32[256,2]{0,1:T(2,128)}, u32[]{:S(2)}) copy-start(s32[256,2]{0,1:T(2,128)} %param.37) | copy-start | bytes 6148
  82.3 26.1 %copy-start.9 = (f32[256,2]{0,1:T(2,128)S(1)}, f32[256,2]{0,1:T(2,128)}, u32[]{:S(2)}) copy-start(f32[256,2]{0,1:T(2,128)} %param.38) | copy-start | bytes 6148
  107.7 1.5 copy-start.1

commit v2 on v1

--- a/solution.py
+++ b/solution.py
@@ -13,6 +13,7 @@
 VB = 128
 BLK = 64
 PAIR = 2
+LANES = 128
 
 
 epsilon = 1e-06
@@ -500,6 +501,419 @@
     )(slots.T, slots, route_weight, residual, gain, gate, up, down)
 
 
+def halves(value):
+    coarse = value.astype(jnp.bfloat16)
+    return coarse, (value - coarse.astype(jnp.float32)).astype(jnp.bfloat16)
+
+
+def contract(left, right, left_axis, right_axis):
+    return lax.dot_general(
+        left,
+        right,
+        (((left_axis,), (right_axis,)), ((), ())),
+        preferred_element_type=jnp.float32,
+    )
+
+
+def rows_by_rows(left, right):
+    (a, b), (c, d) = halves(left), halves(right)
+    return contract(a, c, 1, 1) + (contract(a, d, 1, 1) + contract(b, c, 1, 1))
+
+
+def mixer_kernel(size, tp, *refs):
+    (query_first, key_first, value_first, decay_first, gate_first, norm_first, proj_first) = refs[:7]
+    (query_second, key_second, value_second, decay_second) = refs[7:11]
+    (gate_second, norm_second, proj_second, residual_in, out) = refs[11:16]
+    (projection, attended, early, state, state_sent, state_near, total_sent, total_near) = refs[16:24]
+    (carry_in, carry_out, entering, mixed, part, near, paired, arrived, given, taken) = refs[24:34]
+    sems = refs[34:]
+    recv_sems, up_sems, down_sems, side_sems = sems[:4]
+    state_sems, total_sems, carry_sems, near_sems, cross_sems, row_sems = (
+        sems[4 + 2 * i : 6 + 2 * i] for i in range(6)
+    )
+    pairs, lines, share = tp // PAIR, size // PAIR, size // tp
+    tokens = query_first.shape[0]
+    blocks = tokens // BLK
+    wide_first, wide_second = query_first.shape[1], query_second.shape[1]
+    deep_first, deep_second = value_first.shape[1], value_second.shape[1]
+    cuts = projection.shape[1]
+    height = projection.shape[2]
+    width = part.shape[2]
+    me, mine = lax.axis_index("sp"), lax.axis_index("tp")
+    line, seat = me // PAIR, lax.rem(me, PAIR)
+    sibling = {"tp": tp_member(0, True)}
+    side = {"sp": line * PAIR + lax.rem(seat + 1, PAIR)}
+    above = {"sp": lax.rem(line + 1, lines) * PAIR + seat}
+    below = {"sp": lax.rem(line + lines - 1, lines) * PAIR + seat}
+    greet([side, above, below] + [group_member("tp", tp, step)[2] for step in range(1, tp)])
+    has_above, has_below = line + 1 < lines, line > 0
+
+    def own_piece(p):
+        half = cuts // 2
+        source = proj_first if p < half else proj_second
+        return source.at[pl.ds((p % half) * height, height)]
+
+    def hop(source, chunk, p, send_sems, device):
+        return pltpu.make_async_remote_copy(
+            src_ref=source,
+            dst_ref=projection.at[chunk, p],
+            send_sem=send_sems.at[chunk, p],
+            recv_sem=recv_sems.at[chunk, p],
+            device_id=device,
+            device_id_type=MESH,
+        )
+
+    def relay(chunk, p, send_sems, device):
+        return hop(projection.at[chunk, p], chunk, p, send_sems, device)
+
+    for p in range(cuts):
+
+        @pl.when(has_above)
+        def _():
+            hop(own_piece(p), me, p, up_sems, above).start()
+
+        @pl.when(has_below)
+        def _():
+            hop(own_piece(p), me, p, down_sems, below).start()
+
+        if p < cuts // 2:
+            hop(own_piece(p), me, p, side_sems, side).start()
+
+    own_rows, own_width = taken.shape[1:]
+    for t in range(tp):
+        given[t] = residual_in[:, t * own_width : (t + 1) * own_width]
+
+    def to_owner(step):
+        _, other, device = group_member("tp", tp, step)
+        return remote(given.at[other], taken.at[mine], row_sems, step, device)
+
+    for step in range(1, tp):
+        to_owner(step).start()
+    taken[mine] = given[mine]
+
+    earlier = lax.broadcasted_iota(jnp.int32, (tokens, tokens), 0)
+    later = lax.broadcasted_iota(jnp.int32, (tokens, tokens), 1)
+    causal = (earlier >= later) & (earlier // BLK == later // BLK)
+    lower = jnp.where(causal, 1.0, 0.0).astype(jnp.bfloat16)
+    decay = jnp.concatenate([decay_first[...], decay_second[...]], axis=1)
+    high, low = halves(decay)
+    rest = (decay - high.astype(jnp.float32) - low.astype(jnp.float32)).astype(jnp.bfloat16)
+    running = contract(lower, high, 1, 0) + (contract(lower, low, 1, 0) + contract(lower, rest, 1, 0))
+    ends = [running[(n + 1) * BLK - 1 : (n + 1) * BLK] for n in range(blocks)]
+    before = [jnp.zeros_like(ends[0])]
+    for n in range(blocks):
+        before.append(before[n] + ends[n])
+
+    def spread(parts):
+        shape = (BLK, decay.shape[1])
+        return jnp.concatenate([jnp.broadcast_to(part_row, shape) for part_row in parts], axis=0)
+
+    queries = jnp.concatenate(
+        [
+            query_first[...].astype(jnp.float32) * KA ** (-0.5),
+            query_second[...].astype(jnp.float32) * KB ** (-0.5),
+        ],
+        axis=1,
+    )
+    keys = jnp.concatenate([key_first[...], key_second[...]], axis=1).astype(jnp.float32)
+    decayed = queries * jnp.exp(running)
+    inverse = keys * jnp.exp(-running)
+    to_end = keys * jnp.exp(spread(ends) - running)
+    entry = decayed * jnp.exp(spread(before[:blocks]))
+    early[...] = entry
+    lanes = lax.broadcasted_iota(jnp.int32, (1, LANES), 1)
+
+    heads = []
+    for h in range(wide_first // KA):
+        heads.append((h * KA, None, value_first, h * VA, VA, h * VA, h * VA))
+    for h in range(wide_second // KB):
+        base, inside = h * KB // LANES, h % (LANES // KB)
+        heads.append(
+            (
+                wide_first + base * LANES,
+                inside,
+                value_second,
+                h * VB,
+                VB,
+                deep_first + base * VB,
+                deep_first + h * VB,
+            )
+        )
+
+    def keep(value, inside):
+        if inside is None:
+            return value
+        return jnp.where(lanes // KB == inside, value, 0.0)
+
+    for lane, inside, values, column, depth, _, target in heads:
+        scores = rows_by_rows(
+            keep(decayed[:, lane : lane + LANES], inside), inverse[:, lane : lane + LANES]
+        )
+        a, b = halves(jnp.where(causal, scores, 0.0))
+        value = values[:, column : column + depth]
+        attended[:, target : target + depth] = contract(a, value, 1, 0) + contract(b, value, 1, 0)
+
+    state[...] = jnp.zeros_like(state)
+    for n in range(blocks):
+        span = slice(n * BLK, (n + 1) * BLK)
+        if n:
+            for lane, inside, _, _, depth, row, target in heads:
+                attended[span, target : target + depth] += rows_by_rows(
+                    keep(decayed[span, lane : lane + LANES], inside), state[row : row + depth]
+                )
+        done = set()
+        for lane, inside, values, column, depth, row, _ in heads:
+            a, b = halves(to_end[span, lane : lane + LANES])
+            value = values[span, column : column + depth]
+            added = keep(contract(value, a, 0, 0) + contract(value, b, 0, 0), inside)
+            if row not in done:
+                done.add(row)
+                added = added + state[row : row + depth] * jnp.exp(ends[n][:, lane : lane + LANES])
+                state[row : row + depth] = added
+            else:
+                state[row : row + depth] += added
+
+    state_sent[...] = state[...].astype(jnp.bfloat16)
+    total_sent[...] = jnp.broadcast_to(before[blocks], total_sent.shape)
+    swap_state = remote(state_sent, state_near, state_sems, 0, side)
+    swap_total = remote(total_sent, total_near, total_sems, 0, side)
+    swap_total.start()
+    swap_state.start()
+    for p in range(cuts // 2, cuts):
+        hop(own_piece(p), me, p, side_sems, side).start()
+    for p in range(cuts):
+        projection[me, p] = own_piece(p)[...]
+
+    def faded(total, row, depth, value):
+        lane = row // VA * LANES if row < deep_first else wide_first + (row - deep_first) // VB * LANES
+        return value * jnp.exp(total[:, lane : lane + LANES])
+
+    portions = [(row, VB) for row in range(0, state.shape[0], VB)]
+
+    def carry(i):
+        row, depth = portions[i]
+        return remote(
+            carry_out.at[pl.ds(row, depth)], carry_in.at[pl.ds(row, depth)], carry_sems, i, above
+        )
+
+    def chain():
+        swap_total.wait_recv()
+        swap_state.wait_recv()
+        own_total, other_total = total_sent[0:1, :], total_near[0:1, :]
+
+        @pl.when(line == 0)
+        def _():
+            carry_in[...] = jnp.zeros_like(carry_in)
+
+        lead = (seat == 0).astype(jnp.float32)
+        total_lead = lead * own_total + (1.0 - lead) * other_total
+        total_last = lead * other_total + (1.0 - lead) * own_total
+        for i, (row, depth) in enumerate(portions):
+
+            @pl.when(has_below)
+            def _():
+                carry(i).wait_recv()
+
+            span = slice(row, row + depth)
+            own, other = state[span], state_near[span].astype(jnp.float32)
+            state_lead = lead * own + (1.0 - lead) * other
+            state_last = lead * other + (1.0 - lead) * own
+            come = carry_in[span].astype(jnp.float32)
+            middle = faded(total_lead, row, depth, come) + state_lead
+            carry_out[span] = (faded(total_last, row, depth, middle) + state_last).astype(jnp.bfloat16)
+
+            @pl.when(has_above)
+            def _():
+                carry(i).start()
+
+            entering[span] = lead * come + (1.0 - lead) * middle
+
+    def pass_on(d, c):
+        lower_chunk = jnp.maximum(line - d, 0) * PAIR + seat
+        upper_chunk = jnp.minimum(line + d, lines - 1) * PAIR + seat
+        for p in range(cuts):
+
+            @pl.when(line >= d)
+            def _():
+                hop(projection.at[lower_chunk, p], lower_chunk, p, up_sems, above).wait_recv()
+
+                @pl.when(has_above)
+                def _():
+                    relay(lower_chunk, p, up_sems, above).start()
+
+                relay(lower_chunk, p, side_sems, side).start()
+
+            @pl.when(line + d < lines)
+            def _():
+                relay(upper_chunk, p, down_sems, below).wait_recv()
+
+                @pl.when(has_below)
+                def _():
+                    relay(upper_chunk, p, down_sems, below).start()
+
+                relay(upper_chunk, p, side_sems, side).start()
+
+        @pl.when(d == jnp.clip(line, 1, max(lines - 2, 1)))
+        def _():
+            chain()
+
+        return c
+
+    lax.fori_loop(1, lines, pass_on, 0)
+
+    for lane, inside, _, _, depth, row, target in heads:
+        span = slice(target, target + depth)
+        attention = attended[:, span] + rows_by_rows(
+            keep(early[:, lane : lane + LANES], inside), entering[row : row + depth]
+        )
+        first = target < deep_first
+        gates = gate_first[:, span] if first else gate_second[:, target - deep_first : target - deep_first + depth]
+        gates = gates.astype(jnp.float32)
+        gain = norm_first[...] if first else norm_second[...]
+        scale = lax.rsqrt(jnp.mean(attention * attention, axis=1, keepdims=True) + epsilon)
+        mixed[:, span] = (attention * scale * gain * jax.nn.silu(gates)).astype(jnp.bfloat16)
+
+    def arrive(i, c):
+        chunk = i * PAIR + lax.rem(seat + 1, PAIR)
+        for p in range(cuts):
+            relay(chunk, p, side_sems, side).wait_recv()
+        return c
+
+    lax.fori_loop(0, lines, arrive, 0)
+
+    def project(owner):
+        for i in range(share):
+            chunk = owner * share + i
+            partial_sum = jnp.zeros((tokens, width), jnp.float32)
+            for p in range(cuts):
+                partial_sum = partial_sum + jnp.dot(
+                    mixed[:, p * height : (p + 1) * height],
+                    projection[chunk, p],
+                    preferred_element_type=jnp.float32,
+                )
+            part[chunk] = partial_sum.astype(jnp.bfloat16)
+
+    def to_near(across):
+        return remote(
+            part.at[pl.ds(tp_member(across, True) * share, share)],
+            near.at[across],
+            near_sems,
+            across,
+            sibling,
+        )
+
+    def to_cross(across):
+        return remote(
+            paired.at[across],
+            arrived.at[across],
+            cross_sems,
+            across,
+            {"tp": tp_member(across, False)},
+        )
+
+    hops = list(range(1, pairs)) + [0]
+    for across in hops:
+        project(tp_member(across, True))
+        to_near(across).start()
+        project(tp_member(across, False))
+        if across:
+            to_near(across).wait_recv()
+            for i in range(share):
+                summed = part[tp_member(across, False) * share + i].astype(jnp.float32)
+                paired[across, i] = (summed + near[across, i].astype(jnp.float32)).astype(jnp.bfloat16)
+            to_cross(across).start()
+    for step in range(1, tp):
+        to_owner(step).wait_recv()
+    to_near(0).wait_recv()
+    for across in range(1, pairs):
+        to_cross(across).wait_recv()
+    for i in range(share):
+        summed = part[mine * share + i].astype(jnp.float32) + near[0, i].astype(jnp.float32)
+        for across in range(1, pairs):
+            summed = summed + arrived[across, i].astype(jnp.float32)
+        for t in range(tp):
+            base = taken[t, :, i * width : (i + 1) * width].astype(jnp.float32)
+            rows = slice(t * own_rows, (t + 1) * own_rows)
+            out[rows, i * width : (i + 1) * width] = (base + summed[rows]).astype(jnp.bfloat16)
+
+    swap_state.wait_send()
+    swap_total.wait_send()
+    for i in range(len(portions)):
+
+        @pl.when(has_above)
+        def _():
+            carry(i).wait_send()
+
+    def drain(i, c):
+        chunk = i * PAIR + seat
+        for p in range(cuts):
+            relay(chunk, p, side_sems, side).wait_send()
+
+            @pl.when(has_above & (i <= line))
+            def _():
+                relay(chunk, p, up_sems, above).wait_send()
+
+            @pl.when(has_below & (i >= line))
+            def _():
+                relay(chunk, p, down_sems, below).wait_send()
+
+        return c
+
+    lax.fori_loop(0, lines, drain, 0)
+    for across in range(pairs):
+        to_near(across).wait_send()
+        if across:
+            to_cross(across).wait_send()
+    for step in range(1, tp):
+        to_owner(step).wait_send()
+
+
+def run_mixer(first, second, residual_in, number):
+    size, tp = lax.axis_size("sp"), lax.axis_size("tp")
+    pairs, share = tp // PAIR, size // tp
+    tokens = first[0].shape[0]
+    rows, width = first[-1].shape
+    cuts = 4
+    height = 2 * rows // cuts
+    depth = first[2].shape[1] + second[2].shape[1]
+    keys = first[0].shape[1] + second[0].shape[1]
+    kept = first[2].shape[1] + second[0].shape[1] // LANES * VB
+    own_rows, model = residual_in.shape
+    half, single, dma = jnp.bfloat16, jnp.float32, pltpu.SemaphoreType.DMA
+    return pl.pallas_call(
+        functools.partial(mixer_kernel, size, tp),
+        out_shape=jax.ShapeDtypeStruct((tokens, model // tp), half),
+        in_specs=[VMEM] * 15,
+        out_specs=VMEM,
+        scratch_shapes=[
+            pltpu.VMEM((size, cuts, height, width), half),
+            pltpu.VMEM((tokens, depth), single),
+            pltpu.VMEM((tokens, keys), single),
+            pltpu.VMEM((kept, LANES), single),
+            pltpu.VMEM((kept, LANES), half),
+            pltpu.VMEM((kept, LANES), half),
+            pltpu.VMEM((8, keys), single),
+            pltpu.VMEM((8, keys), single),
+            pltpu.VMEM((kept, LANES), half),
+            pltpu.VMEM((kept, LANES), half),
+            pltpu.VMEM((kept, LANES), single),
+            pltpu.VMEM((tokens, depth), half),
+            pltpu.VMEM((size, tokens, width), half),
+            pltpu.VMEM((pairs, share, tokens, width), half),
+            pltpu.VMEM((pairs, share, tokens, width), half),
+            pltpu.VMEM((pairs, share, tokens, width), half),
+            pltpu.VMEM((tp, own_rows, model // tp), half),
+            pltpu.VMEM((tp, own_rows, model // tp), half),
+        ]
+        + [dma((size, cuts))] * 4
+        + [dma((1,))] * 4
+        + [dma((kept // VB,))] * 2
+        + [dma((pairs,))] * 4
+        + [dma((tp,))] * 2,
+        compiler_params=pltpu.CompilerParams(collective_id=number, has_side_effects=True),
+    )(*first, *second, residual_in)
+
+
 def local_pass(queries, key_rows, values, decay_factors, key_width, value_width):
     count_of_tokens = queries.shape[0]
     head_count = queries.shape[1] // key_width
@@ -567,6 +981,57 @@
     before = jnp.dot(earlier, onehot.astype(jnp.bfloat16), preferred_element_type=jnp.float32)
     ranking = jnp.sum(jnp.where(onehot, before, 0.0), axis=1).astype(jnp.int32)
     return ranking.reshape(block_routes.shape)
+
+
+def plain_mixer(first, second, residual_in):
+    query_first, key_first, value_first, decay_first, gate_first, norm_first, proj_first = first
+    query_second, key_second, value_second, decay_second = second[:4]
+    gate_second, norm_second, proj_second = second[4:]
+    sp_size, tp_size = lax.axis_size("sp"), lax.axis_size("tp")
+    sp_index = lax.axis_index("sp")
+    here = local_pass(query_first, key_first, value_first, decay_first, KA, VA)
+    there = local_pass(query_second, key_second, value_second, decay_second, KB, VB)
+    total_first = jnp.sum(here[3], axis=0).reshape(1, -1)
+    total_second = jnp.sum(there[3], axis=0).reshape(1, -1)
+    totals = jnp.concatenate((total_first, total_second), axis=1)
+    totals = jnp.broadcast_to(totals, (8, totals.shape[1]))
+    all_totals, all_first, all_second, *columns = exchange(
+        (
+            totals,
+            here[4].reshape(-1, VA).astype(jnp.bfloat16),
+            there[4].reshape(-1, VB).astype(jnp.bfloat16),
+            proj_first,
+            proj_second,
+        ),
+        "sp",
+        sp_size,
+        False,
+        0,
+    )
+    columns = [part.transpose(1, 0, 2).reshape(part.shape[1], -1) for part in columns]
+    projection = jnp.concatenate(columns, axis=0)
+    cut = total_first.shape[1]
+    enter_first = entering_state(all_totals[:, 0, :cut], all_first, sp_index)
+    enter_second = entering_state(all_totals[:, 0, cut:], all_second, sp_index)
+    attention_first = finish_pass(*here[:4], enter_first.reshape(here[4].shape))
+    attention_second = finish_pass(*there[:4], enter_second.reshape(there[4].shape))
+    mixed_first = head_norm(attention_first, norm_first, gate_first)
+    mixed_second = head_norm(attention_second, norm_second, gate_second)
+    mixed_rows = jnp.concatenate((mixed_first, mixed_second), axis=1)
+    partial_terms = jnp.dot(mixed_rows, projection, preferred_element_type=jnp.float32)
+    block_tokens = query_first.shape[0]
+    model_width = partial_terms.shape[1]
+    own_tokens = block_tokens // tp_size
+    own_columns = model_width // tp_size
+    by_owner = (block_tokens, tp_size, own_columns)
+    partial_terms = partial_terms.astype(jnp.bfloat16).reshape(by_owner).transpose(1, 0, 2)
+    partial_terms = partial_terms.reshape(tp_size, PAIR, block_tokens // PAIR, own_columns)
+    mixture = reduce_tp(partial_terms, False, 1).reshape(block_tokens, own_columns)
+    own_tokens = residual_in.shape[0]
+    residual = residual_in.reshape(own_tokens, tp_size, own_columns).transpose(1, 0, 2)
+    (residual,) = exchange((residual,), "tp", tp_size, True, 2)
+    residual = residual.reshape(block_tokens, own_columns)
+    return (residual.astype(jnp.float32) + mixture).astype(jnp.bfloat16)
 
 
 def shards(
@@ -593,51 +1058,16 @@
     expert_down,
 ):
     sp_size, tp_size = lax.axis_size("sp"), lax.axis_size("tp")
-    sp_index = lax.axis_index("sp")
-    first = local_pass(query_first, key_first, value_first, decay_first, KA, VA)
-    second = local_pass(query_second, key_second, value_second, decay_second, KB, VB)
-    total_first = jnp.sum(first[3], axis=0).reshape(1, -1)
-    total_second = jnp.sum(second[3], axis=0).reshape(1, -1)
-    totals = jnp.concatenate((total_first, total_second), axis=1)
-    totals = jnp.broadcast_to(totals, (8, totals.shape[1]))
-    all_totals, all_first, all_second, *columns = exchange(
-        (
-            totals,
-            first[4].reshape(-1, VA).astype(jnp.bfloat16),
-            second[4].reshape(-1, VB).astype(jnp.bfloat16),
-            proj_first,
-            proj_second,
-        ),
-        "sp",
-        sp_size,
-        False,
-        0,
-    )
-    columns = [part.transpose(1, 0, 2).reshape(part.shape[1], -1) for part in columns]
-    projection = jnp.concatenate(columns, axis=0)
-    cut = total_first.shape[1]
-    enter_first = entering_state(all_totals[:, 0, :cut], all_first, sp_index)
-    enter_second = entering_state(all_totals[:, 0, cut:], all_second, sp_index)
-    attention_first = finish_pass(*first[:4], enter_first.reshape(first[4].shape))
-    attention_second = finish_pass(*second[:4], enter_second.reshape(second[4].shape))
-    mixed_first = head_norm(attention_first, norm_first, gate_first)
-    mixed_second = head_norm(attention_second, norm_second, gate_second)
-    mixed_rows = jnp.concatenate((mixed_first, mixed_second), axis=1)
-    partial_terms = jnp.dot(mixed_rows, projection, preferred_element_type=jnp.float32)
+    first = (query_first, key_first, value_first, decay_first, gate_first)
+    first += (norm_first.reshape(1, -1), proj_first)
+    second = (query_second, key_second, value_second, decay_second, gate_second)
+    second += (norm_second.reshape(1, -1), proj_second)
+    whole_lanes = proj_first.shape[1] % LANES == 0 and query_second.shape[1] % LANES == 0
+    if whole_lanes and proj_first.shape == proj_second.shape and sp_size % tp_size == 0:
+        residual = run_mixer(first, second, residual_in, 0)
+    else:
+        residual = plain_mixer(first, second, residual_in)
     block_tokens, top_count = route_ids.shape
-    model_width = partial_terms.shape[1]
-    own_tokens = block_tokens // tp_size
-    own_columns = model_width // tp_size
-    by_owner = (block_tokens, tp_size, own_columns)
-    partial_terms = partial_terms.astype(jnp.bfloat16).reshape(by_owner).transpose(1, 0, 2)
-    partial_terms = partial_terms.reshape(tp_size, PAIR, block_tokens // PAIR, own_columns)
-    mixture = reduce_tp(partial_terms, False, 1).reshape(block_tokens, own_columns)
-    own_tokens = residual_in.shape[0]
-    residual = residual_in.reshape(own_tokens, tp_size, own_columns).transpose(1, 0, 2)
-    (residual,) = exchange((residual,), "tp", tp_size, True, 2)
-    residual = residual.reshape(block_tokens, own_columns)
-    residual = (residual.astype(jnp.float32) + mixture).astype(jnp.bfloat16)
-
     experts = sp_size
     capacity = 2 * top_count * block_tokens // experts
     slots = route_ids * capacity + route_positions(route_ids, experts)

time: 207 us -> 129 us (0.62)
  Pallas kernels: 170 us -> 122 us
  local copies, waits for them, and re-layouts: 15.4 us -> 5 us
  other arithmetic: 9.79 us -> 0.71 us
  matrix products: 9.2 us -> 0.34 us
    pallas_call x3 -> x1, Pallas kernels: 76 us -> 44.4 us  [run_mixer(): pl.pallas_call(functools.partial(mixer_kernel, size, tp), out_shape=jax.S...]
    pallas_call x1, Pallas kernels: 93.8 us -> 77.3 us  [run_experts(): pl.pallas_call(functools.partial(experts_kernel, size, tp), out_shape=jax...]
    dot_general x11 -> x0, matrix products: 8.87 us -> none  [the longest x2 2.19 us: finish_pass(): jnp.einsum('nhtd,nhdv->nhtv', query_decayed, states, precision=highest)]
    convert_element_type x5 -> x0, other arithmetic: 4.57 us -> none  [the longest x1 1.88 us: shards(): residual = (residual.astype(jnp.float32) + mixture).astype(jnp.bfloat16)]
    reshape x5 -> x0, local copies, waits for them, and re-layouts: 3.97 us -> none  [the longest x2 2.08 us: arrange(): return source.astype(jnp.float32).reshape(blocks, BLK, head_count, featur...]
    reduce_sum x3 -> x0, other arithmetic: 3.24 us -> none  [the longest x2 3.14 us: entering_state(): return jnp.sum(factor[:, :, None] * states.astype(jnp.float32), axis=0)]
    transpose x3 -> x0, local copies, waits for them, and re-layouts: 3.06 us -> none  [the longest x2 2.03 us: shards(): part.transpose(1, 0, 2).reshape(part.shape[1], -1)]
where the time goes in v2:
time: 129 us; the launch traced here: 128 us
  Pallas kernels  122 us (95%)
  local copies, waits for them, and re-layouts  5 us (4%)
    pallas_call x1, Pallas kernels, run_experts(): pl.pallas_call(functools.partial(experts_kernel, size, tp), out_shape=jax...  77.3 us
    pallas_call x1, Pallas kernels, run_mixer(): pl.pallas_call(functools.partial(mixer_kernel, size, tp), out_shape=jax.S...  44.4 us
    unnamed x5, local copies, waits for them, and re-layouts  3.96 us

profile of v2, /device:TPU:1, one launch (start us, length us, event | category | flops | bytes accessed | tf_op | source)
XLA Modules:
  0.0 127.8 jit_solution(2657488750301172073)
XLA Ops:
  0.0 0.7 broadcast_multiply_fusion
  0.7 0.1 copy.32
  0.8 1.5 %copy.34.route_weight = f32[256,2]{1,0:T(8,128)} copy(f32[256,2]{0,1:T(2,128)} %param.38) | data formatting | bytes 4096 | tf_op args[17]
  2.3 0.8 copy.31
  3.1 0.1 eq.15
  3.3 0.3 fusion
  3.6 0.1 convert_element_type.9
  3.8 0.0 copy-start
  3.8 0.6 copy.33.slots_across
  4.4 44.4 %shard_map.199.residual = bf16[256,512]{1,0:T(8,128)(2,1)} custom-call(bf16[256,128]{1,0:T(8,128)(2,1)} %refs_0_.1, bf16[256,128]{1,0:T(8,128)(2,1)} %refs_1_.1, bf16[256,256]{1,0:T(8,128)(2,1)} %refs_2_.1, f32[256,128]{1,0:T(8,128)} %refs_3_.1, bf16[256,256]{1,0:T(8,128)(2,1)} %refs_4_.1, f32[1,256]{1,0:T(1,128)} %bitcast.12, bf16[256,256]{1,0:T(8,128)(2,1)} %refs_6_.1, ...), custom_call_target="tpu_custom_call" | custom-call | tf_op jit(solution)/shard_map/pallas_call | solution.py:883
  48.9 0.0 copy-done
  48.9 77.3 %shard_map.200 = bf16[64,2048]{1,0:T(8,128)(2,1)} custom-call(s32[2,256]{1,0:T(2,128)} %copy.33.slots_across, s32[256,2]{1,0:T(8,128)} %copy-done, f32[256,2]{1,0:T(8,128)} %copy.34.route_weight, bf16[256,512]{1,0:T(8,128)(2,1)} %shard_map.199.residual, f32[1,2048]{1,0:T(1,128)} %bitcast.11, bf16[2048,896]{1,0:T(8,128)(2,1)} %bitcast.7, ...), custom_call_target="tpu_custom_call" | custom-call | tf_op jit(solution)/shard_map/pallas_call | solution.py:471
  126.2 1.7 %copy.36 = bf16[64,2048]{1,0:T(8,128)(2,1)} copy(bf16[64,2048]{1,0:T(8,128)(2,1)} %shard_map.200) | data formatting | bytes 524288
  (3 shorter events, 0.0 us)
Async XLA Ops:
  3.8 45.1 %copy-start = (s32[256,2]{1,0:T(8,128)}, s32[256,2]{1,0:T(8,128)S(1)}, u32[]{:S(2)}) copy-start(s32[256,2]{1,0:T(8,128)S(1)} %add.14.slots_down) | copy-start | bytes 6148

commit v3 on v2

--- a/solution.py
+++ b/solution.py
@@ -178,22 +178,18 @@
     )(blocks)
 
 
-def ring_offset(step, lines):
-    return lax.rem(step * (lines // 2), lines) + step // 2
-
-
 def experts_kernel(
     size,
     tp,
-    slots_across,
-    slots_down,
+    unit,
+    route_ids,
     route_weight,
     residual,
     gain,
     gate_hbm,
     up_hbm,
     down_hbm,
-    out,
+    collected,
     gate_weights,
     up_weights,
     down_weights,
@@ -209,7 +205,7 @@
     returned,
     total,
     columns,
-    collected,
+    slots_across,
     load_sems,
     *sems,
 ):
@@ -224,12 +220,10 @@
     line, seat = me // PAIR, lax.rem(me, PAIR)
     sibling = {"tp": tp_member(0, True)}
 
-    def forth(k):
-        across = lax.rem(line + ring_offset(k // PAIR, lines), lines)
-        return across * PAIR + lax.rem(seat + lax.rem(k, PAIR), PAIR)
-
-    def back(k):
-        across = lax.rem(line - ring_offset(k // PAIR, lines) + lines, lines)
+    def partner(k):
+        turn = k // PAIR
+        turn = jnp.where(turn > 0, lax.rem(turn, max(lines - 1, 1)) + 1, 0)
+        across = mirrored(line, turn, lines)
         return across * PAIR + lax.rem(seat + lax.rem(k, PAIR), PAIR)
 
     loads = [
@@ -239,17 +233,27 @@
     ]
     for load in loads:
         load.start()
+    numbers = lax.broadcasted_iota(jnp.int32, (size, tokens), 0)
+    hits = [numbers == route_ids[c : c + 1, :] for c in range(route_ids.shape[0])]
+    named = sum(jnp.where(hit, 1.0, 0.0) for hit in hits).astype(jnp.bfloat16)
+    shape = (tokens, tokens)
+    prior = lax.broadcasted_iota(jnp.int32, shape, 0) < lax.broadcasted_iota(jnp.int32, shape, 1)
+    prior = jnp.where(prior, 1.0, 0.0).astype(jnp.bfloat16)
+    counts = jnp.dot(named, prior, preferred_element_type=jnp.float32)
+    for c, hit in enumerate(hits):
+        rank = jnp.sum(jnp.where(hit, counts, 0.0), axis=0, keepdims=True).astype(jnp.int32)
+        slots_across[c : c + 1, :] = route_ids[c : c + 1, :] * capacity + rank
     peers = [group_member("sp", size, step)[2] for step in range(1, size)]
     peers += [group_member("tp", tp, step)[2] for step in range(1, tp)]
     greet(peers)
 
     def outward(k):
         return remote(
-            chosen_rows.at[k], rows.at[me, mine], out_sems, k, {"sp": forth(k)}
+            chosen_rows.at[k], rows.at[me, mine], out_sems, k, {"sp": partner(k)}
         )
 
     def choose(k, target, *index):
-        numbers = lax.broadcasted_iota(jnp.int32, (capacity, tokens), 0) + forth(k) * capacity
+        numbers = lax.broadcasted_iota(jnp.int32, (capacity, tokens), 0) + partner(k) * capacity
         chosen = numbers == slots_across[0:1, :]
         for c in range(1, slots_across.shape[0]):
             chosen = chosen | (numbers == slots_across[c : c + 1, :])
@@ -259,7 +263,9 @@
 
     choose(0, rows, me, mine)
 
-    def send_step(k, carry):
+    def send_step(i, carry):
+        last = i + size - 2 * PAIR
+        k = jnp.where(i < PAIR, i, jnp.where(i < 2 * PAIR, last, i - PAIR))
         choose(k, chosen_rows, k)
         outward(k).start()
         return carry
@@ -267,12 +273,12 @@
     lax.fori_loop(1, size, send_step, 0)
 
     def to_far(k, across):
-        block = rows.at[back(k), mine]
+        block = rows.at[partner(k), mine]
         return remote(block, block, far_sems, (across, k), {"tp": tp_member(across, False)})
 
     def to_pair(k, across):
         origin = tp_member(pairs - across, False) if across else mine
-        block = rows.at[back(k), origin]
+        block = rows.at[partner(k), origin]
         return remote(block, block, pair_sems, (across, k), sibling)
 
     def forward(k):
@@ -281,19 +287,19 @@
         to_pair(k, 0).start()
 
     def forward_group(g):
-        for j in range(PAIR):
-            k = g * PAIR + j
+        for j in range(unit):
+            k = g * unit + j
             outward(k).wait_recv()
             forward(k)
 
     def collect_group(g):
-        for j in range(PAIR):
+        for j in range(unit):
             for across in range(1, pairs):
-                to_far(g * PAIR + j, across).wait_recv()
-                to_pair(g * PAIR + j, across).start()
-        for j in range(PAIR):
+                to_far(g * unit + j, across).wait_recv()
+                to_pair(g * unit + j, across).start()
+        for j in range(unit):
             for across in range(pairs):
-                to_pair(g * PAIR + j, across).wait_recv()
+                to_pair(g * unit + j, across).wait_recv()
 
     def to_near(g, across):
         return remote(
@@ -315,12 +321,12 @@
 
     def homeward(k):
         return remote(
-            done.at[k], returned.at[me], back_sems, k, {"sp": back(k)}
+            done.at[k], returned.at[me], back_sems, k, {"sp": partner(k)}
         )
 
     def run_group(g):
-        for j in range(PAIR):
-            origin = back(g * PAIR + j)
+        for j in range(unit):
+            origin = partner(g * unit + j)
             block = jnp.concatenate([rows[origin, t] for t in range(tp)], axis=1)
             block = block.astype(jnp.float32)
             inverse = lax.rsqrt(jnp.mean(block * block, axis=1, keepdims=True) + epsilon)
@@ -357,20 +363,21 @@
             to_cross(g, across).wait_recv()
             summed = summed + arrived[g, across].astype(jnp.float32)
         summed = summed.astype(jnp.bfloat16)
-        for j in range(PAIR):
+        for j in range(unit):
             part = summed[j * capacity : (j + 1) * capacity]
             if first and j == 0:
                 returned[me] = part
             else:
-                done[g * PAIR + j] = part
-                homeward(g * PAIR + j).start()
+                done[g * unit + j] = part
+                homeward(g * unit + j).start()
 
     forward(0)
-    outward(1).wait_recv()
-    forward(1)
+    for k in range(1, unit):
+        outward(k).wait_recv()
+        forward(k)
     for load in loads:
         load.wait()
-    groups = size // PAIR
+    groups = size // unit
 
     def group_step(g, carry):
         @pl.when(g + 1 < groups)
@@ -380,6 +387,8 @@
         collect_group(g)
         run_group(g)
 
+        cross_group(g)
+
         @pl.when(g == 1)
         def _():
             finish_group(0, True)
@@ -388,24 +397,22 @@
         def _():
             finish_group(g - 1, False)
 
-        cross_group(g)
         return carry
 
     lax.fori_loop(0, groups, group_step, 0)
     finish_group(groups - 1, groups == 1)
 
     def combine(k):
-        expert = forth(k)
-        numbers = lax.broadcasted_iota(jnp.int32, (tokens, capacity), 1) + expert * capacity
-        weights = jnp.zeros((tokens, capacity), jnp.float32)
-        for c in range(route_weight.shape[1]):
+        expert = partner(k)
+        numbers = lax.broadcasted_iota(jnp.int32, (capacity, tokens), 0) + expert * capacity
+        weights = jnp.zeros((capacity, tokens), jnp.float32)
+        for c in range(route_weight.shape[0]):
             weights = weights + jnp.where(
-                numbers == slots_down[:, c : c + 1], route_weight[:, c : c + 1], 0.0
+                numbers == slots_across[c : c + 1, :], route_weight[c : c + 1, :], 0.0
             )
-        coarse = weights.astype(jnp.bfloat16)
-        fine = (weights - coarse.astype(jnp.float32)).astype(jnp.bfloat16)
-        part = jnp.dot(coarse, returned[expert], preferred_element_type=jnp.float32)
-        return part + jnp.dot(fine, returned[expert], preferred_element_type=jnp.float32)
+        coarse, fine = halves(weights)
+        part = contract(coarse, returned[expert], 0, 0)
+        return part + contract(fine, returned[expert], 0, 0)
 
     total[...] = residual[...].astype(jnp.float32) + combine(0)
 
@@ -428,8 +435,6 @@
     collected[mine] = columns[mine]
     for step in range(1, tp):
         to_owner(step).wait_recv()
-    for t in range(tp):
-        out[:, t * width : (t + 1) * width] = collected[t]
 
     def drain_step(k, carry):
         outward(k).wait_send()
@@ -459,19 +464,20 @@
         to_owner(step).wait_send()
 
 
-def run_experts(slots, route_weight, residual, gain, gate, up, down, capacity, number):
+def run_experts(route_ids, route_weight, residual, gain, gate, up, down, capacity, number):
     size, tp = lax.axis_size("sp"), lax.axis_size("tp")
-    pairs, groups = tp // PAIR, size // PAIR
+    unit = 1
+    pairs, groups = tp // PAIR, size // unit
     tokens, width = residual.shape
     model, hidden = gate.shape
     half = jnp.bfloat16
-    taken = PAIR * capacity
+    taken = unit * capacity
     anywhere = pl.BlockSpec(memory_space=pl.ANY)
     dma = pltpu.SemaphoreType.DMA
-    return pl.pallas_call(
-        functools.partial(experts_kernel, size, tp),
-        out_shape=jax.ShapeDtypeStruct((tokens // tp, model), half),
-        in_specs=[VMEM] * 5 + [anywhere] * 3,
+    collected = pl.pallas_call(
+        functools.partial(experts_kernel, size, tp, unit),
+        out_shape=jax.ShapeDtypeStruct((tp, tokens // tp, width), half),
+        in_specs=[VMEM] * 4 + [anywhere] * 3,
         out_specs=VMEM,
         scratch_shapes=[
             pltpu.VMEM(gate.shape, half),
@@ -489,7 +495,7 @@
             pltpu.VMEM((size, capacity, width), half),
             pltpu.VMEM((tokens, width), jnp.float32),
             pltpu.VMEM((tp, tokens // tp, width), half),
-            pltpu.VMEM((tp, tokens // tp, width), half),
+            pltpu.VMEM(route_ids.shape[::-1], jnp.int32),
             dma((3,)),
         ]
         + [dma((size,))] * 2
@@ -498,7 +504,18 @@
         + [dma((size,))] * 2
         + [dma((tp,))] * 2,
         compiler_params=pltpu.CompilerParams(collective_id=number, has_side_effects=True),
-    )(slots.T, slots, route_weight, residual, gain, gate, up, down)
+    )(route_ids.T, route_weight.T, residual, gain, gate, up, down)
+    return collected.transpose(1, 0, 2).reshape(tokens // tp, model)
+
+
+def mirrored(line, step, lines):
+    if lines & (lines - 1):
+        return lax.rem(step + lines - line, lines)
+    place, bit = 0, 1
+    while bit < lines:
+        place = place + lax.rem(line // bit + step // bit, 2) * bit
+        bit = 2 * bit
+    return place
 
 
 def halves(value):
@@ -576,9 +593,9 @@
         def _():
             hop(own_piece(p), me, p, down_sems, below).start()
 
-        if p < cuts // 2:
-            hop(own_piece(p), me, p, side_sems, side).start()
-
+    crossed = cuts - 1
+    for p in (crossed, 0):
+        hop(own_piece(p), me, p, side_sems, side).start()
     own_rows, own_width = taken.shape[1:]
     for t in range(tp):
         given[t] = residual_in[:, t * own_width : (t + 1) * own_width]
@@ -679,8 +696,19 @@
     swap_total = remote(total_sent, total_near, total_sems, 0, side)
     swap_total.start()
     swap_state.start()
-    for p in range(cuts // 2, cuts):
+    for p in range(1, crossed):
         hop(own_piece(p), me, p, side_sems, side).start()
+    beside = line * PAIR + lax.rem(seat + 1, PAIR)
+    relay(beside, crossed, side_sems, side).wait_recv()
+
+    @pl.when(has_above)
+    def _():
+        relay(beside, crossed, up_sems, above).start()
+
+    @pl.when(has_below)
+    def _():
+        relay(beside, crossed, down_sems, below).start()
+
     for p in range(cuts):
         projection[me, p] = own_piece(p)[...]
 
@@ -729,29 +757,34 @@
             entering[span] = lead * come + (1.0 - lead) * middle
 
     def pass_on(d, c):
-        lower_chunk = jnp.maximum(line - d, 0) * PAIR + seat
-        upper_chunk = jnp.minimum(line + d, lines - 1) * PAIR + seat
+        lower_line = jnp.maximum(line - d, 0) * PAIR
+        upper_line = jnp.minimum(line + d, lines - 1) * PAIR
         for p in range(cuts):
-
-            @pl.when(line >= d)
-            def _():
-                hop(projection.at[lower_chunk, p], lower_chunk, p, up_sems, above).wait_recv()
-
-                @pl.when(has_above)
+            for other in range(PAIR if p == crossed else 1):
+                place = lax.rem(seat + other, PAIR)
+                lower_chunk, upper_chunk = lower_line + place, upper_line + place
+
+                @pl.when(line >= d)
                 def _():
-                    relay(lower_chunk, p, up_sems, above).start()
-
-                relay(lower_chunk, p, side_sems, side).start()
-
-            @pl.when(line + d < lines)
-            def _():
-                relay(upper_chunk, p, down_sems, below).wait_recv()
-
-                @pl.when(has_below)
+                    relay(lower_chunk, p, up_sems, above).wait_recv()
+
+                    @pl.when(has_above)
+                    def _():
+                        relay(lower_chunk, p, up_sems, above).start()
+
+                    if p != crossed:
+                        relay(lower_chunk, p, side_sems, side).start()
+
+                @pl.when(line + d < lines)
                 def _():
-                    relay(upper_chunk, p, down_sems, below).start()
-
-                relay(upper_chunk, p, side_sems, side).start()
+                    relay(upper_chunk, p, down_sems, below).wait_recv()
+
+                    @pl.when(has_below)
+                    def _():
+                        relay(upper_chunk, p, down_sems, below).start()
+
+                    if p != crossed:
+                        relay(upper_chunk, p, side_sems, side).start()
 
         @pl.when(d == jnp.clip(line, 1, max(lines - 2, 1)))
         def _():
@@ -773,14 +806,6 @@
         scale = lax.rsqrt(jnp.mean(attention * attention, axis=1, keepdims=True) + epsilon)
         mixed[:, span] = (attention * scale * gain * jax.nn.silu(gates)).astype(jnp.bfloat16)
 
-    def arrive(i, c):
-        chunk = i * PAIR + lax.rem(seat + 1, PAIR)
-        for p in range(cuts):
-            relay(chunk, p, side_sems, side).wait_recv()
-        return c
-
-    lax.fori_loop(0, lines, arrive, 0)
-
     def project(owner):
         for i in range(share):
             chunk = owner * share + i
@@ -811,17 +836,44 @@
             {"tp": tp_member(across, False)},
         )
 
-    hops = list(range(1, pairs)) + [0]
-    for across in hops:
-        project(tp_member(across, True))
-        to_near(across).start()
-        project(tp_member(across, False))
-        if across:
+    tp_seat = lax.rem(mine, PAIR)
+
+    def across_of(owner):
+        return lax.rem(owner // PAIR - mine // PAIR + pairs, pairs)
+
+    def begin(owner):
+        chunk = owner * PAIR + lax.rem(seat + 1, PAIR)
+        for p in range(crossed):
+            relay(chunk, p, side_sems, side).wait_recv()
+        project(owner)
+
+        @pl.when(lax.rem(owner, PAIR) != tp_seat)
+        def _():
+            to_near(across_of(owner)).start()
+
+    def settle(owner):
+        across = across_of(owner)
+
+        @pl.when((lax.rem(owner, PAIR) == tp_seat) & (across > 0))
+        def _():
             to_near(across).wait_recv()
             for i in range(share):
-                summed = part[tp_member(across, False) * share + i].astype(jnp.float32)
+                summed = part[owner * share + i].astype(jnp.float32)
                 paired[across, i] = (summed + near[across, i].astype(jnp.float32)).astype(jnp.bfloat16)
             to_cross(across).start()
+
+    inner = (line > 0) & (line + 1 < lines)
+    owners = []
+    for i in range(tp):
+        place = mirrored(line, i, lines)
+        if 2 <= i and lines == 4:
+            place = jnp.where(inner, mirrored(line, 5 - i, lines), place)
+        owners.append(place)
+    for i in range(tp):
+        begin(owners[i])
+        if i:
+            settle(owners[i - 1])
+    settle(owners[tp - 1])
     for step in range(1, tp):
         to_owner(step).wait_recv()
     to_near(0).wait_recv()
@@ -845,21 +897,24 @@
             carry(i).wait_send()
 
     def drain(i, c):
-        chunk = i * PAIR + seat
         for p in range(cuts):
-            relay(chunk, p, side_sems, side).wait_send()
-
-            @pl.when(has_above & (i <= line))
-            def _():
-                relay(chunk, p, up_sems, above).wait_send()
-
-            @pl.when(has_below & (i >= line))
-            def _():
-                relay(chunk, p, down_sems, below).wait_send()
+            for other in range(PAIR if p == crossed else 1):
+                chunk = i * PAIR + lax.rem(seat + other, PAIR)
+                if p != crossed:
+                    relay(chunk, p, side_sems, side).wait_send()
+
+                @pl.when(has_above & (i <= line))
+                def _():
+                    relay(chunk, p, up_sems, above).wait_send()
+
+                @pl.when(has_below & (i >= line))
+                def _():
+                    relay(chunk, p, down_sems, below).wait_send()
 
         return c
 
     lax.fori_loop(0, lines, drain, 0)
+    relay(me, crossed, side_sems, side).wait_send()
     for across in range(pairs):
         to_near(across).wait_send()
         if across:
@@ -971,16 +1026,6 @@
     gate_silu = jax.nn.silu(gate.astype(jnp.float32).reshape(attention.shape))
     mixed_rows = attention * inverse_rms * head_gain * gate_silu
     return mixed_rows.astype(jnp.bfloat16).reshape(attention.shape[0], -1)
-
-
-def route_positions(block_routes, experts):
-    flattened = block_routes.reshape(-1)
-    amount = flattened.shape[0]
-    onehot = flattened[:, None] == jnp.arange(experts, dtype=jnp.int32)[None, :]
-    earlier = jnp.tril(jnp.ones((amount, amount), jnp.bfloat16), -1)
-    before = jnp.dot(earlier, onehot.astype(jnp.bfloat16), preferred_element_type=jnp.float32)
-    ranking = jnp.sum(jnp.where(onehot, before, 0.0), axis=1).astype(jnp.int32)
-    return ranking.reshape(block_routes.shape)
 
 
 def plain_mixer(first, second, residual_in):
@@ -1063,16 +1108,15 @@
     second = (query_second, key_second, value_second, decay_second, gate_second)
     second += (norm_second.reshape(1, -1), proj_second)
     whole_lanes = proj_first.shape[1] % LANES == 0 and query_second.shape[1] % LANES == 0
-    if whole_lanes and proj_first.shape == proj_second.shape and sp_size % tp_size == 0:
+    if whole_lanes and proj_first.shape == proj_second.shape and sp_size == PAIR * tp_size:
         residual = run_mixer(first, second, residual_in, 0)
     else:
         residual = plain_mixer(first, second, residual_in)
     block_tokens, top_count = route_ids.shape
     experts = sp_size
     capacity = 2 * top_count * block_tokens // experts
-    slots = route_ids * capacity + route_positions(route_ids, experts)
     return run_experts(
-        slots,
+        route_ids,
         route_weight,
         residual,
         expert_norm.reshape(1, -1),

time: 129 us -> 116 us (0.90)
  Pallas kernels: 122 us -> 114 us
  local copies, waits for them, and re-layouts: 5 us -> 1.68 us
    pallas_call x1, Pallas kernels: 44.4 us -> 39.4 us  [run_mixer(): pl.pallas_call(functools.partial(mixer_kernel, size, tp), out_shape=jax.S...]
    unnamed x5 -> x0, local copies, waits for them, and re-layouts: 3.96 us -> none
    pallas_call x1, Pallas kernels: 77.3 us -> 74.3 us  [run_experts(): pl.pallas_call(functools.partial(experts_kernel, size, tp, unit), out_sha...]
    reshape x0 -> x1, local copies, waits for them, and re-layouts: none -> 1.68 us  [run_experts(): return collected.transpose(1, 0, 2).reshape(tokens // tp, model)]
where the time goes in v3:
time: 116 us; the launch traced here: 115 us
  Pallas kernels  114 us (98%)
  local copies, waits for them, and re-layouts  1.68 us (1%)
    pallas_call x1, Pallas kernels, run_experts(): pl.pallas_call(functools.partial(experts_kernel, size, tp, unit), out_sha...  74.3 us
    pallas_call x1, Pallas kernels, run_mixer(): pl.pallas_call(functools.partial(mixer_kernel, size, tp), out_shape=jax.S...  39.4 us

profile of v3, /device:TPU:1, one launch (start us, length us, event | category | flops | bytes accessed | tf_op | source)
XLA Modules:
  0.0 115.4 jit_solution(13325617977990948076)
XLA Ops:
  0.0 39.4 %shard_map.199.residual = bf16[256,512]{1,0:T(8,128)(2,1)} custom-call(bf16[256,128]{1,0:T(8,128)(2,1)} %refs_0_.1, bf16[256,128]{1,0:T(8,128)(2,1)} %refs_1_.1, bf16[256,256]{1,0:T(8,128)(2,1)} %refs_2_.1, f32[256,128]{1,0:T(8,128)} %refs_3_.1, bf16[256,256]{1,0:T(8,128)(2,1)} %refs_4_.1, f32[1,256]{1,0:T(1,128)} %bitcast.18, bf16[256,256]{1,0:T(8,128)(2,1)} %refs_6_.1, ...), custom_call_target="tpu_custom_call" | custom-call | tf_op jit(solution)/shard_map/pallas_call | solution.py:938
  39.4 74.3 %shard_map.200 = bf16[4,64,512]{2,1,0:T(8,128)(2,1)} custom-call(s32[2,256]{1,0:T(2,128)} %bitcast.16, f32[2,256]{1,0:T(2,128)} %bitcast.17, bf16[256,512]{1,0:T(8,128)(2,1)} %shard_map.199.residual, f32[1,2048]{1,0:T(1,128)} %bitcast.15, bf16[2048,896]{1,0:T(8,128)(2,1)} %bitcast.11, bf16[2048,896]{1,0:T(8,128)(2,1)} %bitcast.12, bf16[896,2048]{1,0:T(8,128)(2,1)} %bitcast.13), custom_call_target="tpu_custom_call" | custom-call | tf_op jit(solution)/shard_map/pallas_call | solution.py:477
  113.7 1.7 %copy.23 = bf16[4,8,8,512]{3,2,0,1:T(8,128)(2,1)} copy(bf16[4,8,8,512]{3,2,1,0:T(8,128)(2,1)} %bitcast.14) | data formatting | bytes 524288 | tf_op jit(solution)/shard_map/reshape | solution.py:508
